TPU v7x, 128 devices: a whole 4x4x4 slice. The times are simulated.
128 devices in a mesh: fs: 32 (over z, y, core), tp: 4 (over x).
Axes of the slice: x: 4, y: 4, z: 4, core: 2. Of those that a mesh axis runs over, the one named last changes fastest.
Arguments:
- tokens: bfloat16 [24576, 2048], P('fs'), may hold values from -6 to 6
- norm_gain: float32 [2048], P('fs'), may hold values from 0.1 to 1.9
- gate_weight: float32 [2048, 5632], P('fs', 'tp'), may hold values from -0.125 to 0.125
- up_weight: float32 [2048, 5632], P('fs', 'tp'), may hold values from -0.125 to 0.125
- down_weight: float32 [5632, 2048], P('fs', 'tp'), may hold values from -0.078125 to 0.078125
Outputs:
- gate_out: bfloat16 [2048, 5632], P(None, 'tp')
- up_out: bfloat16 [2048, 5632], P(None, 'tp')
- down_out: bfloat16 [5632, 2048], P('tp')
- mixed: bfloat16 [24576, 2048], P('fs', 'tp')
All inputs are finite; a program needn't handle non-finite values.
Results may differ from a plain program's by a relative error of at most 0.0095.
Values may be sent and summed in bfloat16 or wider, within the bound.
A program may use at most 128 MiB of HBM per device.

v0:
```python
import jax
import jax.numpy as jnp
from jax import lax
from jax.sharding import PartitionSpec as P

eps_norm = 1e-06


def sent_together(arrays, axis, dim, along):
    ends, at = ([], 0)
    for a in arrays[:-1]:
        at += a.shape[along]
        ends.append(at)
    both = jnp.concatenate(arrays, axis=along)
    return tuple(jnp.split(lax.all_gather(both, axis, axis=dim, tiled=True), ends, axis=along))


def on_device(tokens, norm_gain, gate_weight, up_weight, down_weight):
    gain_column = norm_gain[:, None]
    gate_cast = (gate_weight * gain_column).astype(jnp.bfloat16)
    up_cast = (up_weight * gain_column).astype(jnp.bfloat16)
    down_cast = down_weight.astype(jnp.bfloat16)
    gate_out, up_out = sent_together((gate_cast, up_cast), "fs", 0, 1)
    column_block = lax.all_gather(down_cast, "fs", axis=0, tiled=True)
    down_out = lax.all_to_all(column_block, "tp", split_axis=0, concat_axis=1, tiled=True)
    rows_float = tokens.astype(jnp.float32)
    normed = (
        rows_float * lax.rsqrt(jnp.mean(rows_float * rows_float, axis=-1, keepdims=True) + eps_norm)
    ).astype(jnp.bfloat16)
    gate_act = jnp.dot(normed, gate_out, preferred_element_type=jnp.float32)
    up_act = jnp.dot(normed, up_out, preferred_element_type=jnp.float32)
    hidden = (jax.nn.silu(gate_act) * up_act).astype(jnp.bfloat16)
    share = jnp.dot(hidden, down_out, preferred_element_type=jnp.float32).astype(jnp.bfloat16)
    share = lax.optimization_barrier(share).astype(jnp.float32)
    summed = lax.psum_scatter(share.astype(jnp.bfloat16), "tp", scatter_dimension=1, tiled=True)
    return (gate_out, up_out, down_out, summed)


def solution(mesh):
    in_specs = (P("fs", None), P("fs"), P("fs", "tp"), P("fs", "tp"), P("fs", "tp"))
    out_specs = (P(None, "tp"), P(None, "tp"), P("tp", None), P("fs", "tp"))
    return jax.shard_map(
        on_device, mesh=mesh, in_specs=in_specs, out_specs=out_specs, check_vma=False
    )
```

profile of v0, /device:TPU:1, one launch (start us, length us, event | category | flops | bytes accessed | tf_op | source)
XLA Modules:
  0.0 220.8 jit_solution(17548929696489187980)
XLA Ops:
  7.2 0.0 all-gather.5.cloned.1.call-start
  7.2 1.7 convert_element_type.25
  8.9 0.0 all-gather.5.cloned.1.call-update
  8.9 0.0 all-gather.3.cloned.1.call-start
  9.0 1.2 multiply_convert_fusion.2
  10.2 0.8 pad_maximum_fusion
  11.0 0.0 all-gather.3.cloned.1.call-update
  11.0 51.7 %all-gather.5.cloned.1.call-done = bf16[5632,512]{1,0:T(8,128)(2,1)} async-done(((bf16[176,512]{1,0:T(8,128)(2,1)}), bf16[5632,512]{1,0:T(8,128)(2,1)}) %all-gather.5.cloned.1.call-update) | async-done | bytes 5767184 | tf_op jit(solution)/shard_map/all_gather | solution.py:24
  62.7 0.0 copy-start
  62.7 5.4 %all-to-all-start = ((bf16[4,1408,512]{2,1,0:T(8,128)(2,1)}), bf16[4,1408,512]{2,1,0:T(8,128)(2,1)}, u32[]{:S(2)}, u32[]{:S(2)}) async-start(bf16[4,1408,512]{2,1,0:T(8,128)(2,1)} %bitcast.9), calls=%async_computation | async-start | bytes 11534336 | tf_op jit(solution)/shard_map/all_to_all | solution.py:25
  68.1 0.0 reduce-scatter.2.cloned.1.call-start
  68.2 0.0 copy-done
  68.2 0.7 fusion
  68.9 64.8 %all-to-all-done = bf16[4,1408,512]{2,1,0:T(8,128)(2,1)} async-done(((bf16[4,1408,512]{2,1,0:T(8,128)(2,1)}), bf16[4,1408,512]{2,1,0:T(8,128)(2,1)}, u32[]{:S(2)}, u32[]{:S(2)}) %all-to-all-start) | async-done | bytes 5767200 | tf_op jit(solution)/shard_map/all_to_all | solution.py:25
  133.7 8.4 %copy.10 = bf16[4,1408,512]{1,2,0:T(8,128)(2,1)} copy(bf16[4,1408,512]{2,1,0:T(8,128)(2,1)} %all-to-all-done) | data formatting | bytes 11534336 | tf_op jit(solution)/shard_map/all_to_all | solution.py:25
  142.0 0.0 all-gather.3.cloned.1.call-done
  142.0 9.6 %fusion.8 = (bf16[2048,1408]{1,0:T(8,128)(2,1)}, bf16[2048,1408]{1,0:T(8,128)(2,1)}) fusion(bf16[2048,2816]{1,0:T(8,128)(2,1)} %all-gather.3.cloned.1.call-done), kind=kLoop, calls=%fused_computation.12 | loop fusion | bytes 23068672 | tf_op jit(solution)/shard_map/split | solution.py:15
  151.7 9.4 %fusion.3 = f32[768,1408]{1,0:T(8,128)} fusion(bf16[2048,1408]{1,0:T(8,128)(2,1)} %get-tuple-element.9, bf16[768,2048]{1,0:T(8,128)(2,1)S(1)} %copy-done, f32[768]{0:T(1024)S(1)} %add_rsqrt_fusion), kind=kOutput, calls=%fused_computation.6 | convolution fusion | flops 4433903616 | bytes 13241344 | tf_op jit(solution)/shard_map/dot_general | solution.py:30
  161.0 17.3 %convolution_convert_fusion = bf16[768,2048]{1,0:T(8,128)(2,1)} fusion(bf16[1408,2048]{0,1:T(8,128)(2,1)} %bitcast.7, f32[768,1408]{1,0:T(8,128)} %fusion.3, bf16[2048,1408]{1,0:T(8,128)(2,1)} %get-tuple-element.8, bf16[768,2048]{1,0:T(8,128)(2,1)S(1)} %copy-done, f32[768]{0:T(1024)S(1)} %add_rsqrt_fusion), kind=kOutput, calls=%fused_computation.5 | convolution fusion | flops 8871149568 | bytes 22154240 | tf_op jit(solution)/shard_map/dot_general | solution.py:33
  178.4 0.0 reduce-scatter.2.cloned.1.call-update
  178.4 8.4 %copy.11 = bf16[1408,2048]{1,0:T(8,128)(2,1)} copy(bf16[1408,2048]{0,1:T(8,128)(2,1)} %bitcast.8) | data formatting | bytes 11534336
  186.8 27.4 %reduce-scatter.2.cloned.1.call-done = bf16[768,512]{1,0:T(8,128)(2,1)} async-done(((bf16[768,2048]{1,0:T(8,128)(2,1)}), bf16[768,512]{1,0:T(8,128)(2,1)}) %reduce-scatter.2.cloned.1.call-update) | async-done | bytes 786448 | tf_op jit(solution)/shard_map/reduce_scatter | solution.py:35
  (1 shorter events, 0.0 us)
Async XLA Ops:
  7.2 55.5 %all-gather.5.cloned.1.call-start = ((), (), s32[]{:S(2)}) async-start(), calls=%async_computation.3 | async-start | bytes 5947392 | tf_op jit(solution)/shard_map/all_gather | solution.py:24
  8.9 133.1 %all-gather.3.cloned.1.call-start = ((), (), s32[]{:S(2)}) async-start(), calls=%async_computation.2 | async-start | bytes 11894784 | tf_op jit(solution)/shard_map/all_gather | solution.py:15
  62.7 5.5 %copy-start = (bf16[768,2048]{1,0:T(8,128)(2,1)S(1)}, bf16[768,2048]{1,0:T(8,128)(2,1)}, u32[]{:S(2)}) copy-start(bf16[768,2048]{1,0:T(8,128)(2,1)} %param.5) | copy-start | bytes 9437188
  62.7 71.0 %all-to-all-start = ((bf16[4,1408,512]{2,1,0:T(8,128)(2,1)}), bf16[4,1408,512]{2,1,0:T(8,128)(2,1)}, u32[]{:S(2)}, u32[]{:S(2)}) async-start(bf16[4,1408,512]{2,1,0:T(8,128)(2,1)} %bitcast.9), calls=%async_computation | async-start | bytes 11534336 | tf_op jit(solution)/shard_map/all_to_all | solution.py:25
  68.1 146.1 %reduce-scatter.2.cloned.1.call-start = ((), (), s32[]{:S(2)}) async-start(), calls=%async_computation.4 | async-start | bytes 3932160 | tf_op jit(solution)/shard_map/reduce_scatter | solution.py:35
Sparse Core Ops, SparseCore 0:
  10.8 51.8 all-gather.4
  65.5 59.2 all-gather.2
  178.5 35.7 reduce-scatter.1
where the time goes:
time: 221 us
  waiting for transfers between devices  144 us (65%)
  matrix products  26.7 us (12%)
  local copies, waits for them, and re-layouts  26.4 us (12%)
  between operations  13.8 us (6%)
  starting transfers between devices  5.57 us (3%)
  other arithmetic  4.35 us (2%)
    all_to_all x1, waiting for transfers between devices, on_device(): lax.all_to_all(column_block, 'tp', split_axis=0, concat_axis=1, tiled=True)  64.8 us
    all_gather x1, waiting for transfers between devices, on_device(): column_block = lax.all_gather(down_cast, 'fs', axis=0, tiled=True)  51.7 us
    reduce_scatter x1, waiting for transfers between devices, on_device(): lax.psum_scatter(share.astype(jnp.bfloat16), 'tp', scatter_dimension=1, t...  27.4 us
    dot_general x1, matrix products, on_device(): jnp.dot(hidden, down_out, preferred_element_type=jnp.float32)  17.3 us
    split x1, local copies, waits for them, and re-layouts, sent_together(): jnp.split(lax.all_gather(both, axis, axis=dim, tiled=True), ends, axis=al...  9.61 us
    dot_general x1, matrix products, on_device(): gate_act = jnp.dot(normed, gate_out, preferred_element_type=jnp.float32)  9.37 us
    unnamed x3, local copies, waits for them, and re-layouts  8.45 us
    all_to_all x1, local copies, waits for them, and re-layouts, on_device(): lax.all_to_all(column_block, 'tp', split_axis=0, concat_axis=1, tiled=True)  8.36 us
  transfers between devices with their start and end apart: 4, of which 3 were waited for; matrix products, arithmetic and copies ran while one was open for 9% of the time, Pallas kernels for 0%

commit v1 on v0

v1 whole, which is shorter than its diff:
```python
import jax
import jax.numpy as jnp
from jax import lax
from jax.experimental import pallas as pl
from jax.experimental.pallas import tpu as pltpu
from jax.sharding import PartitionSpec as P

MESH = pl.DeviceIdType.MESH
bf16, f32 = jnp.bfloat16, jnp.float32
eps_norm = 1e-06
RING = 4
CHUNKS = ((0, 384), (384, 384), (768, 384), (1152, 256))
NCH = len(CHUNKS)
PIECE = 256
OFFS = ((2, 0), (2, 1), (1, 0), (3, 0), (1, 1), (3, 1), (0, 0), (0, 1))
NP = len(OFFS)
TILE = 256


def ring(v, k):
    return lax.rem(v + k, RING)


def kernel(tok, gain, gw, uw, dw, W, Dn, mixed, X, H, gs, us, ds, dst, gv, S2, S1, R2, R1,
           in_sem, p1s, p1r, p2s, p2r, sbs, sbr, d0s, d0r, d1s, d1r, d2s, d2r, dbs, dbr, rss, rsr):
    x = lax.axis_index("tp")
    f = lax.axis_index("fs")
    c = lax.rem(f, 2)
    y = lax.rem(lax.div(f, 2), RING)
    z = lax.div(f, 2 * RING)
    rows, half = gs.shape[0], gs.shape[0] // 2
    drows, dcols = ds.shape
    dcut = 96

    def at(zz, yy, cc):
        return {"fs": (zz * RING + yy) * 2 + cc}

    zp, zm, yp, ym = ring(z, 1), ring(z, 3), ring(y, 1), ring(y, 3)
    near = ((at(zp, y, c), at(zm, y, c)), (at(z, yp, c), at(z, ym, c)))
    sibling = at(z, y, 1 - c)
    xnear = ({"tp": ring(x, 1)}, {"tp": ring(x, 3)})

    drain = []

    def copy(src, dst, ss, rs, dev):
        return pltpu.make_async_remote_copy(
            src_ref=src, dst_ref=dst, send_sem=ss, recv_sem=rs, device_id=dev, device_id_type=MESH)

    def send(src, dst, ss, rs, dev):
        d = copy(src, dst, ss, rs, dev)
        d.start()
        drain.append((None, d))

    def send_if(cond, src, dst, ss, rs, dev):
        d = copy(src, dst, ss, rs, dev)
        pl.when(cond)(d.start)
        drain.append((cond, d))

    def arrived(region, ss, rs):
        copy(region, region, ss, rs, sibling).wait_recv()

    loads = [pltpu.make_async_copy(s, d, in_sem.at[i])
             for i, (s, d) in enumerate(((gain, gv), (gw, gs), (uw, us), (dw, ds), (tok, X)))]
    for l in loads:
        l.start()
    barrier = pltpu.get_barrier_semaphore()
    greet = [*near[0], *near[1], sibling, {"tp": ring(x, 1)}, {"tp": ring(x, 2)}, {"tp": ring(x, 3)}]
    for dev in greet:
        pl.semaphore_signal(barrier, inc=1, device_id=dev, device_id_type=MESH)

    for l in loads[:3]:
        l.wait()
    eye = lax.broadcasted_iota(jnp.int32, (rows, rows), 0) == lax.broadcasted_iota(jnp.int32, (rows, rows), 1)
    column = jnp.sum(jnp.where(eye, gv[...], 0.0), axis=1, keepdims=True)
    W[0, z, y, c] = (gs[...] * column).astype(bf16)
    W[1, z, y, c] = (us[...] * column).astype(bf16)
    pl.semaphore_wait(barrier, len(greet))

    def region(a, first, second, part=None, k=None):
        zz, yy = (ring(z, first), ring(y, second)) if a == 0 else (ring(z, second), ring(y, first))
        cols = slice(None) if k is None else pl.ds(*CHUNKS[k])
        lead = slice(None) if part is None else part
        return W.at[lead, zz, yy, c, pl.ds(a * half, half), cols]

    def row_of(a, second, core, k):
        cols = pl.ds(*CHUNKS[k])
        if a == 0:
            return W.at[:, :, ring(y, second), core, pl.ds(0, half), cols]
        return W.at[:, ring(z, second), :, core, pl.ds(half, half), cols]

    def p1_send():
        for d in (0, 1):
            for a in (0, 1):
                r = region(a, 0, 0)
                send(r, r, p1s.at[a, d], p1r.at[a, d], near[a][d])

    def p1_forward():
        for d in (0, 1):
            for a in (0, 1):
                arrived(region(a, 3 - 2 * d, 0), p1s.at[a, d], p1r.at[a, d])
                r = region(a, 3 - 2 * d, 0, d)
                send(r, r, p1s.at[a, 2 + d], p1r.at[a, 2 + d], near[a][d])

    def p1_finish():
        for d in (0, 1):
            for a in (0, 1):
                arrived(region(a, 2, 0, d), p1s.at[a, 2 + d], p1r.at[a, 2 + d])

    def p2_send(k, js):
        for j in js:
            for d in (0, 1):
                for a in (0, 1):
                    r = region(a, j, 0, None, k)
                    send(r, r, p2s.at[k, a, d, j], p2r.at[k, a, d, j], near[1 - a][d])

    def p2_forward(k):
        for j in (0, 1, 3, 2):
            for d in (0, 1):
                for a in (0, 1):
                    arrived(region(a, j, 3 - 2 * d, None, k), p2s.at[k, a, d, j], p2r.at[k, a, d, j])
                    r = region(a, j, 3 - 2 * d, d, k)
                    send(r, r, p2s.at[k, a, 2 + d, j], p2r.at[k, a, 2 + d, j], near[1 - a][d])

    def p2_finish(k):
        for j in (0, 1, 3, 2):
            for d in (0, 1):
                for a in (0, 1):
                    arrived(region(a, j, 2, d, k), p2s.at[k, a, 2 + d, j], p2r.at[k, a, 2 + d, j])

    def sib_send(k, seconds):
        for s in seconds:
            for a in (0, 1):
                r = row_of(a, s, c, k)
                send(r, r, sbs.at[k, a, s], sbr.at[k, a, s], sibling)

    def sib_finish(k):
        for s in range(RING):
            for a in (0, 1):
                arrived(row_of(a, s, 1 - c, k), sbs.at[k, a, s], sbr.at[k, a, s])

    def hidden(k):
        start, width = CHUNKS[k]

        def body(t, _):
            at_rows = pl.ds(pl.multiple_of(t * TILE, TILE), TILE)
            a = X[at_rows, :]
            wg = W[0, :, :, :, :, pl.ds(start, width)].reshape(-1, width)
            wu = W[1, :, :, :, :, pl.ds(start, width)].reshape(-1, width)
            g = jnp.dot(a, wg, preferred_element_type=f32)
            u = jnp.dot(a, wu, preferred_element_type=f32)
            H[at_rows, pl.ds(start, width)] = (g / (1.0 + jnp.exp(-g)) * u).astype(bf16)
            return 0

        lax.fori_loop(0, X.shape[0] // TILE, body, 0)

    def place(q):
        return pl.multiple_of(q * dcols, dcols)

    def piece_cols(i):
        off, p = OFFS[i]
        return pl.ds(pl.multiple_of(ring(x, off) * dcols + p * PIECE, PIECE), PIECE)

    def d0_send():
        loads[3].wait()
        mine = pl.ds(place(x), dcols)
        own = ds[...].astype(bf16)
        dst[...] = own

        @pl.when(x == z)
        def _():
            Dn[y, c, :, mine] = own

        send_if(x != z, dst, Dn.at[y, c, :, mine], d0s.at[0], d0r.at[x], {"tp": z})

    def d0_finish():
        for k in (1, 2, 3):
            q = ring(x, k)
            pl.when(x == z)(lambda q=q: arrived(Dn.at[y, c, :, pl.ds(place(q), dcols)], d0s.at[0], d0r.at[q]))

    lo, hi = pl.ds(0, dcut), pl.ds(dcut, drows - dcut)
    cuts = (lo, hi)

    def d1_send(i):
        r = Dn.at[y, c, :, piece_cols(i)]
        for d in (0, 1):
            send_if(z == x, r, r, d1s.at[i, d], d1r.at[i, d], near[0][d])

    def d1_forward(i):
        cols = piece_cols(i)
        for d in (0, 1):
            here = z == ring(x, 1 + 2 * d)
            pl.when(here)(lambda d=d: arrived(Dn.at[y, c, :, cols], d1s.at[i, d], d1r.at[i, d]))
            r = Dn.at[y, c, cuts[d], cols]
            send_if(here, r, r, d1s.at[i, 2 + d], d1r.at[i, 2 + d], near[0][d])
        for d in (0, 1):
            pl.when(z == ring(x, 2))(
                lambda d=d: arrived(Dn.at[y, c, cuts[d], cols], d1s.at[i, 2 + d], d1r.at[i, 2 + d]))

    def d2_send(i):
        r = Dn.at[y, c, :, piece_cols(i)]
        for d in (0, 1):
            send(r, r, d2s.at[i, d], d2r.at[i, d], near[1][d])

    def d2_forward(i):
        cols = piece_cols(i)
        for d in (0, 1):
            yy = ring(y, 3 - 2 * d)
            arrived(Dn.at[yy, c, :, cols], d2s.at[i, d], d2r.at[i, d])
            r = Dn.at[yy, c, cuts[d], cols]
            send(r, r, d2s.at[i, 2 + d], d2r.at[i, 2 + d], near[1][d])

    def d2_finish(i):
        cols = piece_cols(i)
        for d in (0, 1):
            arrived(Dn.at[ring(y, 2), c, cuts[d], cols], d2s.at[i, 2 + d], d2r.at[i, 2 + d])
        r = Dn.at[:, c, :, cols]
        send(r, r, dbs.at[i], dbr.at[i], sibling)

    def d_ready(i):
        arrived(Dn.at[:, 1 - c, :, piece_cols(i)], dbs.at[i], dbr.at[i])

    def share(i):
        off, p = OFFS[i]
        cols = piece_cols(i)
        hw = PIECE // 2
        if off == 1:
            arrived(R2.at[p, 0], rss.at[0, p, 0], rsr.at[0, p, 0])
        if off == 3:
            arrived(R2.at[p, 1], rss.at[0, p, 1], rsr.at[0, p, 1])
        if off == 0:
            for d in (0, 1):
                arrived(R1.at[p, d], rss.at[1, p, d], rsr.at[1, p, d])

        def body(t, _):
            at_rows = pl.ds(pl.multiple_of(t * TILE, TILE), TILE)
            w = Dn[:, :, :, cols].reshape(-1, PIECE)
            v = jnp.dot(H[at_rows, :], w, preferred_element_type=f32)
            if off == 2:
                v = v.astype(bf16)
                S2[p, 0, at_rows, :] = v[:, hw:]
                S2[p, 1, at_rows, :] = v[:, :hw]
            elif off == 1:
                S1[p, 0, at_rows, pl.ds(0, hw)] = v[:, :hw].astype(bf16)
                S1[p, 0, at_rows, pl.ds(hw, hw)] = (v[:, hw:] + R2[p, 0, at_rows, :].astype(f32)).astype(bf16)
            elif off == 3:
                S1[p, 1, at_rows, pl.ds(0, hw)] = (v[:, :hw] + R2[p, 1, at_rows, :].astype(f32)).astype(bf16)
                S1[p, 1, at_rows, pl.ds(hw, hw)] = v[:, hw:].astype(bf16)
            else:
                v = v + R1[p, 0, at_rows, :].astype(f32) + R1[p, 1, at_rows, :].astype(f32)
                mixed[at_rows, pl.ds(p * PIECE, PIECE)] = v.astype(bf16)
            return 0

        lax.fori_loop(0, H.shape[0] // TILE, body, 0)
        if off == 2:
            for d in (0, 1):
                send(S2.at[p, d], R2.at[p, d], rss.at[0, p, d], rsr.at[0, p, d], xnear[d])
        if off in (1, 3):
            d = (off - 1) // 2
            send(S1.at[p, d], R1.at[p, d], rss.at[1, p, d], rsr.at[1, p, d], xnear[d])

    def norm():
        loads[4].wait()
        step = 32

        def body(t, _):
            at_rows = pl.ds(pl.multiple_of(t * step, step), step)
            v = X[at_rows, :].astype(f32)
            m = jnp.mean(v * v, axis=-1, keepdims=True)
            X[at_rows, :] = (v * lax.rsqrt(m + eps_norm)).astype(bf16)
            return 0

        lax.fori_loop(0, X.shape[0] // step, body, 0)

    p1_send()
    p2_send(0, (0,))
    p2_send(1, (0,))
    d0_send()
    norm()
    p1_forward()
    p2_send(0, (1, 3))
    p2_send(1, (1, 3))
    p1_finish()
    p2_send(0, (2,))
    p2_send(1, (2,))
    p2_send(2, (0,))
    d0_finish()
    for k in range(NCH):
        p2_forward(k)
        sib_send(k, (0, 1, 3))
        if k + 2 < NCH:
            p2_send(k + 2, (1, 3, 2))
        if k + 3 < NCH:
            p2_send(k + 3, (0,))
        if k == NCH - 2:
            d1_send(0)
            d1_send(1)
        if k == NCH - 1:
            d1_forward(0)
            d2_send(0)
            for i in range(2, NP):
                d1_send(i)
        if k:
            sib_finish(k - 1)
            hidden(k - 1)
        p2_finish(k)
        sib_send(k, (2,))
    d1_forward(1)
    d2_send(1)
    d2_forward(0)
    sib_finish(NCH - 1)
    hidden(NCH - 1)
    d2_finish(0)
    for i in range(NP):
        if i + 2 < NP:
            d1_forward(i + 2)
            d2_send(i + 2)
        if i + 1 < NP:
            d2_forward(i + 1)
            d2_finish(i + 1)
        d_ready(i)
        share(i)
    for cond, d in drain:
        if cond is None:
            d.wait_send()
        else:
            pl.when(cond)(d.wait_send)


def write_out(W, Dn, m, g_out, u_out, d_out, m_out, sem):
    copies = [pltpu.make_async_copy(s, d, sem.at[i])
              for i, (s, d) in enumerate(((W.at[0], g_out), (W.at[1], u_out), (Dn, d_out), (m, m_out)))]
    for c in copies:
        c.start()
    for c in copies:
        c.wait()


def on_device(tokens, norm_gain, gate_weight, up_weight, down_weight):
    toks, width = tokens.shape
    rows, ff = gate_weight.shape
    drows, dcols = down_weight.shape
    hbm = pl.BlockSpec(memory_space=pltpu.HBM)
    vmem = pl.BlockSpec(memory_space=pltpu.VMEM)
    dma = pltpu.SemaphoreType.DMA
    half_piece = PIECE // 2
    W, Dn, m = pl.pallas_call(
        kernel,
        out_shape=(
            pltpu.VMEM((2, RING, RING, 2, rows, ff), bf16),
            pltpu.VMEM((RING, 2, drows, width), bf16),
            pltpu.VMEM((toks, dcols), bf16),
        ),
        in_specs=[hbm] * 5,
        out_specs=(vmem,) * 3,
        scratch_shapes=[
            pltpu.VMEM((toks, width), bf16),
            pltpu.VMEM((toks, ff), bf16),
            pltpu.VMEM((rows, ff), f32),
            pltpu.VMEM((rows, ff), f32),
            pltpu.VMEM((drows, dcols), f32),
            pltpu.VMEM((drows, dcols), bf16),
            pltpu.VMEM((1, rows), f32),
            pltpu.VMEM((2, 2, toks, half_piece), bf16),
            pltpu.VMEM((2, 2, toks, PIECE), bf16),
            pltpu.VMEM((2, 2, toks, half_piece), bf16),
            pltpu.VMEM((2, 2, toks, PIECE), bf16),
            dma((5,)),
            dma((2, 4)), dma((2, 4)),
            dma((NCH, 2, 4, RING)), dma((NCH, 2, 4, RING)),
            dma((NCH, 2, RING)), dma((NCH, 2, RING)),
            dma((1,)), dma((RING,)),
            dma((NP, 4)), dma((NP, 4)),
            dma((NP, 4)), dma((NP, 4)),
            dma((NP,)), dma((NP,)),
            dma((2, 2, 2)), dma((2, 2, 2)),
        ],
        compiler_params=pltpu.CompilerParams(
            collective_id=0, has_side_effects=True, vmem_limit_bytes=36 * 2**20),
    )(tokens, norm_gain.reshape(1, rows), gate_weight, up_weight, down_weight)
    return pl.pallas_call(
        write_out,
        out_shape=(
            jax.ShapeDtypeStruct((width, ff), bf16),
            jax.ShapeDtypeStruct((width, ff), bf16),
            jax.ShapeDtypeStruct((ff, width), bf16),
            jax.ShapeDtypeStruct((toks, dcols), bf16),
        ),
        in_specs=[vmem] * 3,
        out_specs=(hbm,) * 4,
        scratch_shapes=[dma((4,))],
        compiler_params=pltpu.CompilerParams(vmem_limit_bytes=2**20),
    )(W.reshape(2, width, ff), Dn.reshape(ff, width), m)


def solution(mesh):
    in_specs = (P("fs", None), P("fs"), P("fs", "tp"), P("fs", "tp"), P("fs", "tp"))
    out_specs = (P(None, "tp"), P(None, "tp"), P("tp", None), P("fs", "tp"))
    return jax.shard_map(
        on_device, mesh=mesh, in_specs=in_specs, out_specs=out_specs, check_vma=False
    )
```

time: 221 us -> 111 us (0.50)
  the two profiles are of different devices: /device:TPU:1 before, /device:TPU:2 now
where the time goes in v1:
time: 111 us
  Pallas kernels  109 us (98%)
  local copies, waits for them, and re-layouts  1.63 us (1%)
    pallas_call x1, Pallas kernels, on_device(): pl.pallas_call(kernel, out_shape=(pltpu.VMEM((2, RING, RING, 2, rows, ff)...  102 us
    pallas_call x1, Pallas kernels, on_device(): pl.pallas_call(write_out, out_shape=(jax.ShapeDtypeStruct((width, ff), bf...  6.28 us

profile of v1, /device:TPU:2, one launch (start us, length us, event | category | flops | bytes accessed | tf_op | source)
XLA Modules:
  0.0 111.0 jit_solution(8072105181252807597)
XLA Ops:
  0.6 0.0 copy-start
  0.6 1.0 copy-done
  1.6 0.0 copy-start.1
  1.6 0.7 copy-done.1
  2.3 102.4 %shard_map.84 = (bf16[2,4,4,2,64,1408]{5,4,3,2,1,0:T(8,128)(2,1)S(1)}, bf16[4,2,176,2048]{3,2,1,0:T(8,128)(2,1)S(1)}, bf16[768,512]{1,0:T(8,128)(2,1)S(1)}) custom-call(bf16[768,2048]{1,0:T(8,128)(2,1)} %tok.1, f32[1,64]{1,0:T(1,128)S(1)} %bitcast.5, f32[64,1408]{1,0:T(8,128)S(1)} %copy-done, f32[64,1408]{1,0:T(8,128)} %uw.1, f32[176,512]{1,0:T(8,128)} %dw.1), custom_call_target="tpu_custom_call" | custom-call | tf_op jit(solution)/shard_map/pallas_call | solution.py:346
  104.7 6.3 %shard_map.85 = (bf16[2048,1408]{1,0:T(8,128)(2,1)}, bf16[2048,1408]{1,0:T(8,128)(2,1)}, bf16[1408,2048]{1,0:T(8,128)(2,1)}, bf16[768,512]{1,0:T(8,128)(2,1)}) custom-call(bf16[2,2048,1408]{2,1,0:T(8,128)(2,1)S(1)} %bitcast.3, bf16[1408,2048]{1,0:T(8,128)(2,1)S(1)} %bitcast.4, bf16[768,512]{1,0:T(8,128)(2,1)S(1)} %get-tuple-element.9.m), custom_call_target="tpu_custom_call" | custom-call | tf_op jit(solution)/shard_map/pallas_call | solution.py:380
Async XLA Ops:
  0.6 1.0 copy-start
  1.6 0.7 copy-start.1

commit v2 on v1

--- a/solution.py
+++ b/solution.py
@@ -11,10 +11,23 @@
 RING = 4
 CHUNKS = ((0, 384), (384, 384), (768, 384), (1152, 256))
 NCH = len(CHUNKS)
+PARTS = 3
 PIECE = 256
 OFFS = ((2, 0), (2, 1), (1, 0), (3, 0), (1, 1), (3, 1), (0, 0), (0, 1))
 NP = len(OFFS)
 TILE = 256
+ORDER = (
+    "P1S", "P2S.1.0", "P2S.0.0", "P1F", "D0S", "NORM.0", "P2S.2.0", "P2S.0.3", "P2S.1.1", "P2S.0.1",
+    "P2S.2.1", "P1E", "P2S.1.2", "P2S.1.3", "P2S.2.2", "P2S.3.0", "P2S.0.2", "NORM.1", "P2S.2.3", "D0",
+    "D1S.0", "P2F.1", "P2F.0", "D1F.0", "P2F.2", "P2E.1", "P2S.3.1", "P2S.3.3", "P2S.3.2", "D1E.0", "D1S.1",
+    "NORM.2", "P2E.0", "HID.1.0", "D1S.2", "D2S.0", "P2E.2", "HID.0.0", "HID.0.1", "P2F.3", "D1S.3",
+    "HID.1.1", "D2F.0", "D1S.4", "D1F.1", "HID.2.0", "HID.0.2", "D1F.2", "D2E.0", "D1S.5", "HID.2.1",
+    "D1E.1", "D2S.1", "D1S.6", "P2E.3", "HID.1.2", "D1E.2", "D1F.3", "HID.3.0", "D2S.2", "D1S.7", "HID.2.2",
+    "D1F.4", "HID.3.1", "D2F.1", "D1E.3", "HID.3.2", "D2S.3", "SH.0", "D1E.4", "D2F.2", "D1F.5", "D2E.1",
+    "D2S.4", "D1F.6", "D2F.3", "SH.1", "D2E.2", "D1E.5", "D1E.6", "D2F.4", "D2S.5", "D1F.7", "D2S.6",
+    "D2E.3", "SH.2", "SH.3", "D2E.4", "D2F.5", "D1E.7", "SH.4", "D2S.7", "D2F.6", "D2E.5", "SH.5", "D2F.7",
+    "D2E.7", "D2E.6", "SH.6", "SH.7",
+)
 
 
 def ring(v, k):
@@ -76,82 +89,84 @@
     W[1, z, y, c] = (us[...] * column).astype(bf16)
     pl.semaphore_wait(barrier, len(greet))
 
+    def cols_of(k):
+        return slice(None) if k is None else pl.ds(*CHUNKS[k])
+
     def region(a, first, second, part=None, k=None):
         zz, yy = (ring(z, first), ring(y, second)) if a == 0 else (ring(z, second), ring(y, first))
-        cols = slice(None) if k is None else pl.ds(*CHUNKS[k])
         lead = slice(None) if part is None else part
-        return W.at[lead, zz, yy, c, pl.ds(a * half, half), cols]
-
-    def row_of(a, second, core, k):
-        cols = pl.ds(*CHUNKS[k])
+        return W.at[lead, zz, yy, c, pl.ds(a * half, half), cols_of(k)]
+
+    def line(a, second, core, k, part=None):
+        lead = slice(None) if part is None else part
         if a == 0:
-            return W.at[:, :, ring(y, second), core, pl.ds(0, half), cols]
-        return W.at[:, ring(z, second), :, core, pl.ds(half, half), cols]
-
-    def p1_send():
-        for d in (0, 1):
-            for a in (0, 1):
-                r = region(a, 0, 0)
-                send(r, r, p1s.at[a, d], p1r.at[a, d], near[a][d])
-
-    def p1_forward():
+            return W.at[lead, :, ring(y, second), core, pl.ds(0, half), cols_of(k)]
+        return W.at[lead, ring(z, second), :, core, pl.ds(half, half), cols_of(k)]
+
+    def begin(src, ss, rs, dev):
+        copy(src, src, ss, rs, dev).start()
+
+    def sent(region_sent, ss):
+        drain.append((None, copy(region_sent, region_sent, ss, ss, sibling)))
+
+    def P1S():
+        for d in (0, 1):
+            for a in (0, 1):
+                begin(region(a, 0, 0), p1s.at[a, d], p1r.at[a, d], near[a][d])
+                sent(region(a, 0, 0), p1s.at[a, d])
+
+    def P1F():
         for d in (0, 1):
             for a in (0, 1):
                 arrived(region(a, 3 - 2 * d, 0), p1s.at[a, d], p1r.at[a, d])
                 r = region(a, 3 - 2 * d, 0, d)
-                send(r, r, p1s.at[a, 2 + d], p1r.at[a, 2 + d], near[a][d])
-
-    def p1_finish():
+                begin(r, p1s.at[a, 2 + d], p1r.at[a, 2 + d], near[a][d])
+                sent(r, p1s.at[a, 2 + d])
+
+    def P1E():
         for d in (0, 1):
             for a in (0, 1):
                 arrived(region(a, 2, 0, d), p1s.at[a, 2 + d], p1r.at[a, 2 + d])
 
-    def p2_send(k, js):
-        for j in js:
-            for d in (0, 1):
-                for a in (0, 1):
-                    r = region(a, j, 0, None, k)
-                    send(r, r, p2s.at[k, a, d, j], p2r.at[k, a, d, j], near[1 - a][d])
-
-    def p2_forward(k):
-        for j in (0, 1, 3, 2):
-            for d in (0, 1):
-                for a in (0, 1):
-                    arrived(region(a, j, 3 - 2 * d, None, k), p2s.at[k, a, d, j], p2r.at[k, a, d, j])
-                    r = region(a, j, 3 - 2 * d, d, k)
-                    send(r, r, p2s.at[k, a, 2 + d, j], p2r.at[k, a, 2 + d, j], near[1 - a][d])
-
-    def p2_finish(k):
-        for j in (0, 1, 3, 2):
-            for d in (0, 1):
-                for a in (0, 1):
-                    arrived(region(a, j, 2, d, k), p2s.at[k, a, 2 + d, j], p2r.at[k, a, 2 + d, j])
-
-    def sib_send(k, seconds):
-        for s in seconds:
-            for a in (0, 1):
-                r = row_of(a, s, c, k)
-                send(r, r, sbs.at[k, a, s], sbr.at[k, a, s], sibling)
-
-    def sib_finish(k):
-        for s in range(RING):
-            for a in (0, 1):
-                arrived(row_of(a, s, 1 - c, k), sbs.at[k, a, s], sbr.at[k, a, s])
-
-    def hidden(k):
+    def P2S(k, j):
+        for d in (0, 1):
+            for a in (0, 1):
+                begin(region(a, j, 0, None, k), p2s.at[k, a, d], p2r.at[k, a, d], near[1 - a][d])
+                if j == 0:
+                    sent(line(a, 0, c, k), p2s.at[k, a, d])
+
+    def sib(k, second):
+        for a in (0, 1):
+            begin(line(a, second, c, k), sbs.at[k], sbr.at[k], sibling)
+
+    def P2F(k):
+        for d in (0, 1):
+            for a in (0, 1):
+                arrived(line(a, 3 - 2 * d, c, k), p2s.at[k, a, d], p2r.at[k, a, d])
+                r = line(a, 3 - 2 * d, c, k, d)
+                begin(r, p2s.at[k, a, 2 + d], p2r.at[k, a, 2 + d], near[1 - a][d])
+                sent(r, p2s.at[k, a, 2 + d])
+        for second in (0, 1, 3):
+            sib(k, second)
+
+    def P2E(k):
+        for d in (0, 1):
+            for a in (0, 1):
+                arrived(line(a, 2, c, k, d), p2s.at[k, a, 2 + d], p2r.at[k, a, 2 + d])
+        sib(k, 2)
+        sent(W.at[:, :, :, c, :, cols_of(k)], sbs.at[k])
+
+    def HID(k, t):
+        if t == 0:
+            arrived(W.at[:, :, :, 1 - c, :, cols_of(k)], sbs.at[k], sbr.at[k])
         start, width = CHUNKS[k]
-
-        def body(t, _):
-            at_rows = pl.ds(pl.multiple_of(t * TILE, TILE), TILE)
-            a = X[at_rows, :]
-            wg = W[0, :, :, :, :, pl.ds(start, width)].reshape(-1, width)
-            wu = W[1, :, :, :, :, pl.ds(start, width)].reshape(-1, width)
-            g = jnp.dot(a, wg, preferred_element_type=f32)
-            u = jnp.dot(a, wu, preferred_element_type=f32)
-            H[at_rows, pl.ds(start, width)] = (g / (1.0 + jnp.exp(-g)) * u).astype(bf16)
-            return 0
-
-        lax.fori_loop(0, X.shape[0] // TILE, body, 0)
+        tile = X.shape[0] // PARTS
+        at_rows = pl.ds(t * tile, tile)
+        cols = pl.ds(start, width)
+        w = jnp.concatenate([W[0, :, :, :, :, cols].reshape(-1, width), W[1, :, :, :, :, cols].reshape(-1, width)], axis=1)
+        v = jnp.dot(X[at_rows, :], w, preferred_element_type=f32)
+        g, u = v[:, :width], v[:, width:]
+        H[at_rows, cols] = (g / (1.0 + jnp.exp(-g)) * u).astype(bf16)
 
     def place(q):
         return pl.multiple_of(q * dcols, dcols)
@@ -160,7 +175,7 @@
         off, p = OFFS[i]
         return pl.ds(pl.multiple_of(ring(x, off) * dcols + p * PIECE, PIECE), PIECE)
 
-    def d0_send():
+    def D0S():
         loads[3].wait()
         mine = pl.ds(place(x), dcols)
         own = ds[...].astype(bf16)
@@ -172,7 +187,7 @@
 
         send_if(x != z, dst, Dn.at[y, c, :, mine], d0s.at[0], d0r.at[x], {"tp": z})
 
-    def d0_finish():
+    def D0():
         for k in (1, 2, 3):
             q = ring(x, k)
             pl.when(x == z)(lambda q=q: arrived(Dn.at[y, c, :, pl.ds(place(q), dcols)], d0s.at[0], d0r.at[q]))
@@ -180,46 +195,53 @@
     lo, hi = pl.ds(0, dcut), pl.ds(dcut, drows - dcut)
     cuts = (lo, hi)
 
-    def d1_send(i):
-        r = Dn.at[y, c, :, piece_cols(i)]
-        for d in (0, 1):
-            send_if(z == x, r, r, d1s.at[i, d], d1r.at[i, d], near[0][d])
-
-    def d1_forward(i):
-        cols = piece_cols(i)
+    def all_sent(i, cond, r, ss):
+        if i == NP - 1:
+            drain.append((cond, copy(r, r, ss, ss, sibling)))
+
+    def D1S(i):
+        for d in (0, 1):
+            r = Dn.at[y, c, :, piece_cols(i)]
+            pl.when(z == x)(copy(r, r, d1s.at[d], d1r.at[i, d], near[0][d]).start)
+            all_sent(i, z == x, Dn.at[y, c, :, :], d1s.at[d])
+
+    def D1F(i):
         for d in (0, 1):
             here = z == ring(x, 1 + 2 * d)
-            pl.when(here)(lambda d=d: arrived(Dn.at[y, c, :, cols], d1s.at[i, d], d1r.at[i, d]))
-            r = Dn.at[y, c, cuts[d], cols]
-            send_if(here, r, r, d1s.at[i, 2 + d], d1r.at[i, 2 + d], near[0][d])
-        for d in (0, 1):
-            pl.when(z == ring(x, 2))(
-                lambda d=d: arrived(Dn.at[y, c, cuts[d], cols], d1s.at[i, 2 + d], d1r.at[i, 2 + d]))
-
-    def d2_send(i):
-        r = Dn.at[y, c, :, piece_cols(i)]
-        for d in (0, 1):
-            send(r, r, d2s.at[i, d], d2r.at[i, d], near[1][d])
-
-    def d2_forward(i):
-        cols = piece_cols(i)
+
+            @pl.when(here)
+            def _():
+                arrived(Dn.at[y, c, :, piece_cols(i)], d1s.at[d], d1r.at[i, d])
+                begin(Dn.at[y, c, cuts[d], piece_cols(i)], d1s.at[2 + d], d1r.at[i, 2 + d], near[0][d])
+
+            all_sent(i, here, Dn.at[y, c, cuts[d], :], d1s.at[2 + d])
+
+    def D1E(i):
+        @pl.when(z == ring(x, 2))
+        def _():
+            for d in (0, 1):
+                arrived(Dn.at[y, c, cuts[d], piece_cols(i)], d1s.at[2 + d], d1r.at[i, 2 + d])
+
+    def D2S(i):
+        for d in (0, 1):
+            begin(Dn.at[y, c, :, piece_cols(i)], d2s.at[d], d2r.at[i, d], near[1][d])
+            all_sent(i, None, Dn.at[y, c, :, :], d2s.at[d])
+
+    def D2F(i):
         for d in (0, 1):
             yy = ring(y, 3 - 2 * d)
-            arrived(Dn.at[yy, c, :, cols], d2s.at[i, d], d2r.at[i, d])
-            r = Dn.at[yy, c, cuts[d], cols]
-            send(r, r, d2s.at[i, 2 + d], d2r.at[i, 2 + d], near[1][d])
-
-    def d2_finish(i):
-        cols = piece_cols(i)
-        for d in (0, 1):
-            arrived(Dn.at[ring(y, 2), c, cuts[d], cols], d2s.at[i, 2 + d], d2r.at[i, 2 + d])
-        r = Dn.at[:, c, :, cols]
-        send(r, r, dbs.at[i], dbr.at[i], sibling)
-
-    def d_ready(i):
-        arrived(Dn.at[:, 1 - c, :, piece_cols(i)], dbs.at[i], dbr.at[i])
-
-    def share(i):
+            arrived(Dn.at[yy, c, :, piece_cols(i)], d2s.at[d], d2r.at[i, d])
+            begin(Dn.at[yy, c, cuts[d], piece_cols(i)], d2s.at[2 + d], d2r.at[i, 2 + d], near[1][d])
+            all_sent(i, None, Dn.at[yy, c, cuts[d], :], d2s.at[2 + d])
+
+    def D2E(i):
+        for d in (0, 1):
+            arrived(Dn.at[ring(y, 2), c, cuts[d], piece_cols(i)], d2s.at[2 + d], d2r.at[i, 2 + d])
+        begin(Dn.at[:, c, :, piece_cols(i)], dbs.at[0], dbr.at[i], sibling)
+        all_sent(i, None, Dn.at[:, c, :, :], dbs.at[0])
+
+    def SH(i):
+        arrived(Dn.at[:, 1 - c, :, piece_cols(i)], dbs.at[0], dbr.at[i])
         off, p = OFFS[i]
         cols = piece_cols(i)
         hw = PIECE // 2
@@ -258,67 +280,25 @@
             d = (off - 1) // 2
             send(S1.at[p, d], R1.at[p, d], rss.at[1, p, d], rsr.at[1, p, d], xnear[d])
 
-    def norm():
-        loads[4].wait()
+    def NORM(t):
+        if t == 0:
+            loads[4].wait()
         step = 32
-
-        def body(t, _):
-            at_rows = pl.ds(pl.multiple_of(t * step, step), step)
+        count = X.shape[0] // 3 // step
+
+        def body(i, _):
+            at_rows = pl.ds(pl.multiple_of((t * count + i) * step, step), step)
             v = X[at_rows, :].astype(f32)
             m = jnp.mean(v * v, axis=-1, keepdims=True)
             X[at_rows, :] = (v * lax.rsqrt(m + eps_norm)).astype(bf16)
             return 0
 
-        lax.fori_loop(0, X.shape[0] // step, body, 0)
-
-    p1_send()
-    p2_send(0, (0,))
-    p2_send(1, (0,))
-    d0_send()
-    norm()
-    p1_forward()
-    p2_send(0, (1, 3))
-    p2_send(1, (1, 3))
-    p1_finish()
-    p2_send(0, (2,))
-    p2_send(1, (2,))
-    p2_send(2, (0,))
-    d0_finish()
-    for k in range(NCH):
-        p2_forward(k)
-        sib_send(k, (0, 1, 3))
-        if k + 2 < NCH:
-            p2_send(k + 2, (1, 3, 2))
-        if k + 3 < NCH:
-            p2_send(k + 3, (0,))
-        if k == NCH - 2:
-            d1_send(0)
-            d1_send(1)
-        if k == NCH - 1:
-            d1_forward(0)
-            d2_send(0)
-            for i in range(2, NP):
-                d1_send(i)
-        if k:
-            sib_finish(k - 1)
-            hidden(k - 1)
-        p2_finish(k)
-        sib_send(k, (2,))
-    d1_forward(1)
-    d2_send(1)
-    d2_forward(0)
-    sib_finish(NCH - 1)
-    hidden(NCH - 1)
-    d2_finish(0)
-    for i in range(NP):
-        if i + 2 < NP:
-            d1_forward(i + 2)
-            d2_send(i + 2)
-        if i + 1 < NP:
-            d2_forward(i + 1)
-            d2_finish(i + 1)
-        d_ready(i)
-        share(i)
+        lax.fori_loop(0, count, body, 0)
+
+    does = {f.__name__: f for f in (P1S, P1F, P1E, P2S, P2F, P2E, HID, NORM, D0S, D0, D1S, D1F, D1E, D2S, D2F, D2E, SH)}
+    for word in ORDER:
+        name, *numbers = word.split(".")
+        does[name](*map(int, numbers))
     for cond, d in drain:
         if cond is None:
             d.wait_send()
@@ -366,16 +346,16 @@
             pltpu.VMEM((2, 2, toks, PIECE), bf16),
             dma((5,)),
             dma((2, 4)), dma((2, 4)),
-            dma((NCH, 2, 4, RING)), dma((NCH, 2, 4, RING)),
-            dma((NCH, 2, RING)), dma((NCH, 2, RING)),
+            dma((NCH, 2, 4)), dma((NCH, 2, 4)),
+            dma((NCH,)), dma((NCH,)),
             dma((1,)), dma((RING,)),
-            dma((NP, 4)), dma((NP, 4)),
-            dma((NP, 4)), dma((NP, 4)),
-            dma((NP,)), dma((NP,)),
+            dma((4,)), dma((NP, 4)),
+            dma((4,)), dma((NP, 4)),
+            dma((1,)), dma((NP,)),
             dma((2, 2, 2)), dma((2, 2, 2)),
         ],
         compiler_params=pltpu.CompilerParams(
-            collective_id=0, has_side_effects=True, vmem_limit_bytes=36 * 2**20),
+            collective_id=0, has_side_effects=True, vmem_limit_bytes=48_900_000),
     )(tokens, norm_gain.reshape(1, rows), gate_weight, up_weight, down_weight)
     return pl.pallas_call(
         write_out,

time: 111 us -> 90.8 us (0.82)
  the two profiles are of different devices: /device:TPU:2 before, /device:TPU:1 now
where the time goes in v2:
time: 90.8 us; the launch traced here: 90.7 us
  Pallas kernels  90 us (99%)
    pallas_call x1, Pallas kernels, on_device(): pl.pallas_call(kernel, out_shape=(pltpu.VMEM((2, RING, RING, 2, rows, ff)...  83.7 us
    pallas_call x1, Pallas kernels, on_device(): pl.pallas_call(write_out, out_shape=(jax.ShapeDtypeStruct((width, ff), bf...  6.28 us

profile of v2, /device:TPU:1, one launch (start us, length us, event | category | flops | bytes accessed | tf_op | source)
XLA Modules:
  0.0 90.7 jit_solution(12685529009137575154)
XLA Ops:
  0.6 83.7 %shard_map.84 = (bf16[2,4,4,2,64,1408]{5,4,3,2,1,0:T(8,128)(2,1)S(1)}, bf16[4,2,176,2048]{3,2,1,0:T(8,128)(2,1)S(1)}, bf16[768,512]{1,0:T(8,128)(2,1)S(1)}) custom-call(bf16[768,2048]{1,0:T(8,128)(2,1)} %tok.1, f32[1,64]{1,0:T(1,128)} %bitcast.5, f32[64,1408]{1,0:T(8,128)} %gw.1, f32[64,1408]{1,0:T(8,128)} %uw.1, f32[176,512]{1,0:T(8,128)} %dw.1), custom_call_target="tpu_custom_call" | custom-call | tf_op jit(solution)/shard_map/pallas_call | solution.py:326
  84.4 6.3 %shard_map.85 = (bf16[2048,1408]{1,0:T(8,128)(2,1)}, bf16[2048,1408]{1,0:T(8,128)(2,1)}, bf16[1408,2048]{1,0:T(8,128)(2,1)}, bf16[768,512]{1,0:T(8,128)(2,1)}) custom-call(bf16[2,2048,1408]{2,1,0:T(8,128)(2,1)S(1)} %bitcast.3, bf16[1408,2048]{1,0:T(8,128)(2,1)S(1)} %bitcast.4, bf16[768,512]{1,0:T(8,128)(2,1)S(1)} %get-tuple-element.9.m), custom_call_target="tpu_custom_call" | custom-call | tf_op jit(solution)/shard_map/pallas_call | solution.py:360

commit v3 on v2

v3 whole, which is shorter than its diff:
```python
import jax
import jax.numpy as jnp
from jax import lax
from jax.experimental import pallas as pl
from jax.experimental.pallas import tpu as pltpu
from jax.sharding import PartitionSpec as P

MESH = pl.DeviceIdType.MESH
bf16, f32 = jnp.bfloat16, jnp.float32
eps_norm = 1e-06
RING = 4
CHUNKS = ((0, 384), (384, 256), (640, 256), (896, 256), (1152, 256))
NCH = len(CHUNKS)
PARTS = 2
PIECE = 256
OFFS = ((2, 0), (2, 1), (1, 0), (3, 0), (1, 1), (3, 1), (0, 0), (0, 1))
NP = len(OFFS)
TILE = 256
ORDER = (
    "P1S.0", "P1S.1", "P1S.2", "P2S.0.0", "P1S.3", "P2S.4.0", "P2S.3.0", "D0S.0", "NORM.0", "P1S.4",
    "P1F.0", "P1F.2", "P2S.2.3", "P2S.0.3", "P1F.4", "P2S.2.0", "P1E.0", "P1E.2", "D0S.1", "P1F.3",
    "P2S.0.1", "P2S.4.1", "NORM.1", "P2S.2.1", "P2S.0.2", "D0.0", "P1F.1", "NORM.2", "P2S.1.3", "D1S.0",
    "P1E.4", "P2S.4.2", "P2S.4.3", "P1E.1", "P2S.2.2", "P2F.0", "P2S.1.1", "D0.1", "D1F.0", "P2S.1.2",
    "D1S.1", "P2S.3.3", "P2E.0", "P2S.1.0", "P2F.4", "P2S.3.1", "P1E.3", "P2S.3.2", "D1E.0", "D1F.1",
    "D2S.0", "P2F.2", "HID.0.0", "P2E.4", "D1E.1", "D1S.2", "D2S.1", "P2F.3", "HID.0.1", "P2E.2", "D1S.3",
    "D2F.0", "P2F.1", "HID.4.0", "D1S.4", "D1F.2", "HID.4.1", "HID.2.0", "D2F.1", "P2E.3", "D1S.5",
    "HID.2.1", "D1F.3", "D1E.2", "D2S.2", "D2E.0", "HID.3.0", "P2E.1", "HID.3.1", "D1S.6", "D1S.7", "D1E.3",
    "D2S.3", "D2E.1", "HID.1.0", "HID.1.1", "D1F.4", "SH.0", "D1F.5", "D2F.2", "SH.1", "D2F.3", "D1E.4",
    "D2S.4", "D1F.6", "D1F.7", "D2E.2", "D1E.5", "D2S.5", "D2E.3", "D1E.6", "D2S.6", "SH.2", "SH.3",
    "D2F.4", "D1E.7", "D2S.7", "D2F.5", "D2F.6", "D2E.4", "D2F.7", "SH.4", "D2E.5", "D2E.6", "D2E.7",
    "SH.5", "SH.6", "SH.7",
)


def ring(v, k):
    return lax.rem(v + k, RING)


def kernel(tok, gain, gw, uw, dw, W, Dn, H, R1, Tp, Tm, X, gs, us, ds, dst, gv, S2, S1, R2,
           in_sem, out_sem, sib_sem, gu_sem, d0_sem, d_sem, r2_sem, r1_sem):
    x = lax.axis_index("tp")
    f = lax.axis_index("fs")
    c = lax.rem(f, 2)
    y = lax.rem(lax.div(f, 2), RING)
    z = lax.div(f, 2 * RING)
    rows, half = gs.shape[0], gs.shape[0] // 2
    drows, dcols = ds.shape
    dcut = 96

    def at(zz, yy, cc):
        return {"fs": (zz * RING + yy) * 2 + cc}

    zp, zm, yp, ym = ring(z, 1), ring(z, 3), ring(y, 1), ring(y, 3)
    near = ((at(zp, y, c), at(zm, y, c)), (at(z, yp, c), at(z, ym, c)))
    sibling = at(z, y, 1 - c)
    xnear = ({"tp": ring(x, 1)}, {"tp": ring(x, 3)})

    drain = []

    def copy(src, dst, ss, rs, dev):
        return pltpu.make_async_remote_copy(
            src_ref=src, dst_ref=dst, send_sem=ss, recv_sem=rs, device_id=dev, device_id_type=MESH)

    def begin(src, ss, rs, dev):
        copy(src, src, ss, rs, dev).start()

    def arrived(view, rs):
        copy(view, view, out_sem.at[0], rs, sibling).wait_recv()

    def sent(view, ss, cond=None):
        drain.append((cond, copy(view, view, ss, ss, sibling)))

    loads = [pltpu.make_async_copy(s, d, in_sem.at[i])
             for i, (s, d) in enumerate(((gain, gv), (gw, gs), (uw, us), (dw, ds), (tok, X)))]
    for l in loads:
        l.start()
    barrier = pltpu.get_barrier_semaphore()
    greet = [*near[0], *near[1], sibling, {"tp": ring(x, 1)}, {"tp": ring(x, 2)}, {"tp": ring(x, 3)}]
    for dev in greet:
        pl.semaphore_signal(barrier, inc=1, device_id=dev, device_id_type=MESH)

    for l in loads[:3]:
        l.wait()
    eye = lax.broadcasted_iota(jnp.int32, (rows, rows), 0) == lax.broadcasted_iota(jnp.int32, (rows, rows), 1)
    column = jnp.sum(jnp.where(eye, gv[...], 0.0), axis=1, keepdims=True)
    W[0, z, y, c] = (gs[...] * column).astype(bf16)
    W[1, z, y, c] = (us[...] * column).astype(bf16)
    pl.semaphore_wait(barrier, len(greet))

    def cols_of(k):
        return pl.ds(*CHUNKS[k])

    def region(a, first, second, part, k):
        zz, yy = (ring(z, first), ring(y, second)) if a == 0 else (ring(z, second), ring(y, first))
        lead = slice(None) if part is None else part
        return W.at[lead, zz, yy, c, pl.ds(a * half, half), cols_of(k)]

    def line(a, second, core, k, part=None):
        lead = slice(None) if part is None else part
        if a == 0:
            return W.at[lead, :, ring(y, second), core, pl.ds(0, half), cols_of(k)]
        return W.at[lead, ring(z, second), :, core, pl.ds(half, half), cols_of(k)]

    def P1S(k):
        for d in (0, 1):
            for a in (0, 1):
                begin(region(a, 0, 0, None, k), out_sem.at[0], gu_sem.at[k, 0], near[a][d])
        if k == 0:
            sent(W.at[:, 0, 0], out_sem.at[0])

    def P1F(k):
        arrived(W.at[:, 0, 0, :, :, cols_of(k)], gu_sem.at[k, 0])
        for d in (0, 1):
            for a in (0, 1):
                begin(region(a, 3 - 2 * d, 0, d, k), out_sem.at[1], gu_sem.at[k, 1], near[a][d])
        if k == 0:
            sent(W.at[0, 0, 0], out_sem.at[1])

    def P1E(k):
        arrived(W.at[0, 0, 0, :, :, cols_of(k)], gu_sem.at[k, 1])

    def P2S(k, j):
        for d in (0, 1):
            for a in (0, 1):
                begin(region(a, j, 0, None, k), out_sem.at[2], gu_sem.at[k, 2], near[1 - a][d])
        if k == 0 and j == 0:
            sent(W.at[:, :, 0], out_sem.at[2])

    def sib(k, second):
        for a in (0, 1):
            begin(line(a, second, c, k), sib_sem.at[0, k], sib_sem.at[1, k], sibling)

    def P2F(k):
        arrived(W.at[:, :, 0, :, :, cols_of(k)], gu_sem.at[k, 2])
        for d in (0, 1):
            for a in (0, 1):
                begin(line(a, 3 - 2 * d, c, k, d), out_sem.at[3], gu_sem.at[k, 3], near[1 - a][d])
        if k == 0:
            sent(W.at[0, :, 0], out_sem.at[3])
        for second in (0, 1, 3):
            sib(k, second)

    def P2E(k):
        arrived(W.at[0, :, 0, :, :, cols_of(k)], gu_sem.at[k, 3])
        sib(k, 2)
        sent(W.at[:, :, :, c, :, cols_of(k)], sib_sem.at[0, k])

    def HID(k, t):
        if t == 0:
            arrived(W.at[:, :, :, 1 - c, :, cols_of(k)], sib_sem.at[1, k])
        start, width = CHUNKS[k]
        tile = X.shape[0] // PARTS
        at_rows = pl.ds(t * tile, tile)
        cols = pl.ds(start, width)
        w = jnp.concatenate([W[0, :, :, :, :, cols].reshape(-1, width), W[1, :, :, :, :, cols].reshape(-1, width)], axis=1)
        v = jnp.dot(X[at_rows, :], w, preferred_element_type=f32)
        g, u = v[:, :width], v[:, width:]
        H[at_rows, cols] = (g / (1.0 + jnp.exp(-g)) * u).astype(bf16)

    def place(q):
        return pl.multiple_of(q * dcols, dcols)

    def piece_cols(i):
        off, p = OFFS[i]
        return pl.ds(pl.multiple_of(ring(x, off) * dcols + p * PIECE, PIECE), PIECE)

    def D0S(late):
        mine = pl.ds(place(x), dcols)
        if not late:
            loads[3].wait()
            rounded = ds[...].astype(bf16)
            dst[...] = rounded

            @pl.when(x == z)
            def _():
                Dn[y, c, :, mine] = rounded

        go = (z == ring(x, 1)) | (z == ring(x, 3)) if late else z == ring(x, 2)
        pl.when(go)(copy(dst, Dn.at[y, c, :, mine], out_sem.at[4], d0_sem.at[late], {"tp": z}).start)
        if late:
            sent(dst, out_sem.at[4], z != x)

    def D0(late):
        @pl.when(x == z)
        def _():
            arrived(Dn.at[y, c, :, pl.ds(0, (1 + late) * dcols)], d0_sem.at[late])

    lo, hi = pl.ds(0, dcut), pl.ds(dcut, drows - dcut)
    cuts = (lo, hi)

    def D1S(i):
        r = Dn.at[y, c, :, piece_cols(i)]

        @pl.when(z == x)
        def _():
            for d in (0, 1):
                begin(r, out_sem.at[5], d_sem.at[0, i], near[0][d])

        if i == 0:
            sent(Dn.at[0:2, c], out_sem.at[5], z == x)

    def D1F(i):
        for d in (0, 1):
            here = z == ring(x, 1 + 2 * d)

            @pl.when(here)
            def _():
                arrived(Dn.at[y, c, :, piece_cols(i)], d_sem.at[0, i])
                begin(Dn.at[y, c, cuts[d], piece_cols(i)], out_sem.at[6], d_sem.at[1, i], near[0][d])

            if i == 0:
                sent(Dn.at[y, c, cuts[d]], out_sem.at[6], here)

    def D1E(i):
        @pl.when(z == ring(x, 2))
        def _():
            arrived(Dn.at[y, c, :, piece_cols(i)], d_sem.at[1, i])

    def D2S(i):
        for d in (0, 1):
            begin(Dn.at[y, c, :, piece_cols(i)], out_sem.at[7], d_sem.at[2, i], near[1][d])
        if i == 0:
            sent(Dn.at[0:2, c], out_sem.at[7])

    def D2F(i):
        arrived(Dn.at[0:2, c, :, piece_cols(i)], d_sem.at[2, i])
        for d in (0, 1):
            begin(Dn.at[ring(y, 3 - 2 * d), c, cuts[d], piece_cols(i)], out_sem.at[8], d_sem.at[3, i], near[1][d])
        if i == 0:
            sent(Dn.at[y, c], out_sem.at[8])

    def D2E(i):
        arrived(Dn.at[y, c, :, piece_cols(i)], d_sem.at[3, i])
        begin(Dn.at[:, c, :, piece_cols(i)], out_sem.at[9], d_sem.at[4, i], sibling)
        if i == 0:
            sent(Dn.at[:, c], out_sem.at[9])

    def SH(i):
        arrived(Dn.at[:, 1 - c, :, piece_cols(i)], d_sem.at[4, i])
        off, p = OFFS[i]
        if off == 0:
            return
        d = (off - 1) // 2
        cols = piece_cols(i)
        hw = PIECE // 2
        if off != 2:
            arrived(R2.at[p, d], r2_sem.at[p, d])

        def body(t, _):
            at_rows = pl.ds(pl.multiple_of(t * TILE, TILE), TILE)
            w = Dn[:, :, :, cols].reshape(-1, PIECE)
            v = jnp.dot(H[at_rows, :], w, preferred_element_type=f32)
            if off == 2:
                v = v.astype(bf16)
                S2[p, 0, at_rows, :] = v[:, hw:]
                S2[p, 1, at_rows, :] = v[:, :hw]
                for e in (0, 1):
                    copy(S2.at[p, e, at_rows, :], R2.at[p, e, at_rows, :],
                         out_sem.at[10], r2_sem.at[p, e], xnear[e]).start()
                return 0
            plain, added = pl.ds(d * hw, hw), pl.ds((1 - d) * hw, hw)
            to = S1.at[d] if p == 0 else (Tp, Tm)[d]
            to[at_rows, plain] = v[:, d * hw:(d + 1) * hw].astype(bf16)
            to[at_rows, added] = (
                v[:, (1 - d) * hw:(2 - d) * hw] + R2[p, d, at_rows, :].astype(f32)).astype(bf16)
            if p == 0:
                copy(S1.at[d, at_rows, :], R1.at[d, at_rows, :], out_sem.at[11], r1_sem.at[0], xnear[d]).start()
            return 0

        lax.fori_loop(0, H.shape[0] // TILE, body, 0)
        if i == 0:
            sent(S2, out_sem.at[10])
            sent(S1, out_sem.at[11])

    def NORM(t):
        if t == 0:
            loads[4].wait()
        step = 128
        count = X.shape[0] // 3 // step

        def body(i, _):
            at_rows = pl.ds(pl.multiple_of((t * count + i) * step, step), step)
            v = X[at_rows, :].astype(f32)
            m = jnp.mean(v * v, axis=-1, keepdims=True)
            X[at_rows, :] = (v * lax.rsqrt(m + eps_norm)).astype(bf16)
            return 0

        lax.fori_loop(0, count, body, 0)

    does = {f.__name__: f for f in (P1S, P1F, P1E, P2S, P2F, P2E, HID, NORM, D0S, D0, D1S, D1F, D1E, D2S, D2F, D2E, SH)}
    for word in ORDER:
        name, *numbers = word.split(".")
        does[name](*map(int, numbers))
    arrived(R1, r1_sem.at[0])
    for cond, d in drain:
        if cond is None:
            d.wait_send()
        else:
            pl.when(cond)(d.wait_send)


def write_out(W, Dn, H, R1, g_out, u_out, d_out, done, own, sem):
    x = lax.axis_index("tp")
    ff, width = d_out.shape
    dcols = width // RING
    copies = []
    for src, out in ((W.at[0], g_out), (W.at[1], u_out), (Dn, d_out)):
        n = out.shape[0] // 4
        for i in range(4):
            r = pl.ds(i * n, n)
            copies.append(pltpu.make_async_copy(src.at[r], out.at[r], sem.at[len(copies)]))
    for cp in copies:
        cp.start()

    def body(t, _):
        at_rows = pl.ds(pl.multiple_of(t * TILE, TILE), TILE)
        w = Dn[:, pl.ds(pl.multiple_of(x * dcols, dcols), dcols)]
        v = jnp.dot(H[at_rows, :], w, preferred_element_type=f32)
        v0 = v[:, :PIECE] + R1[0, at_rows, :].astype(f32) + R1[1, at_rows, :].astype(f32)
        done[at_rows, :] = v0.astype(bf16)
        own[at_rows, :] = v[:, PIECE:]
        return 0

    lax.fori_loop(0, H.shape[0] // TILE, body, 0)
    for cp in copies:
        cp.wait()


def add_last(done, own, up, down, m_out, last, sem):
    copies = [pltpu.make_async_copy(done, m_out.at[:, pl.ds(0, PIECE)], sem.at[0]),
              pltpu.make_async_copy(last, m_out.at[:, pl.ds(PIECE, PIECE)], sem.at[1])]
    copies[0].start()
    last[...] = (own[...] + up[...].astype(f32) + down[...].astype(f32)).astype(bf16)
    copies[1].start()
    for cp in copies:
        cp.wait()


def on_device(tokens, norm_gain, gate_weight, up_weight, down_weight):
    toks, width = tokens.shape
    rows, ff = gate_weight.shape
    drows, dcols = down_weight.shape
    hbm = pl.BlockSpec(memory_space=pltpu.HBM)
    vmem = pl.BlockSpec(memory_space=pltpu.VMEM)
    dma = pltpu.SemaphoreType.DMA
    half_piece = PIECE // 2
    W, Dn, H, R1, Tp, Tm = pl.pallas_call(
        kernel,
        out_shape=(
            pltpu.VMEM((2, RING, RING, 2, rows, ff), bf16),
            pltpu.VMEM((RING, 2, drows, width), bf16),
            pltpu.VMEM((toks, ff), bf16),
            pltpu.VMEM((2, toks, PIECE), bf16),
            pltpu.VMEM((toks, PIECE), bf16),
            pltpu.VMEM((toks, PIECE), bf16),
        ),
        in_specs=[hbm] * 5,
        out_specs=(vmem,) * 6,
        scratch_shapes=[
            pltpu.VMEM((toks, width), bf16),
            pltpu.VMEM((rows, ff), f32),
            pltpu.VMEM((rows, ff), f32),
            pltpu.VMEM((drows, dcols), f32),
            pltpu.VMEM((drows, dcols), bf16),
            pltpu.VMEM((1, rows), f32),
            pltpu.VMEM((2, 2, toks, half_piece), bf16),
            pltpu.VMEM((2, toks, PIECE), bf16),
            pltpu.VMEM((2, 2, toks, half_piece), bf16),
            dma((5,)),
            dma((12,)),
            dma((2, NCH)),
            dma((NCH, 4)),
            dma((2,)),
            dma((5, NP)),
            dma((2, 2)),
            dma((1,)),
        ],
        compiler_params=pltpu.CompilerParams(
            collective_id=0, has_side_effects=True, vmem_limit_bytes=45_800_000),
    )(tokens, norm_gain.reshape(1, rows), gate_weight, up_weight, down_weight)
    up = lax.ppermute(Tp, "tp", [(i, (i + 1) % RING) for i in range(RING)])
    down = lax.ppermute(Tm, "tp", [(i, (i + RING - 1) % RING) for i in range(RING)])
    g_out, u_out, d_out, done, own = pl.pallas_call(
        write_out,
        out_shape=(
            jax.ShapeDtypeStruct((width, ff), bf16),
            jax.ShapeDtypeStruct((width, ff), bf16),
            jax.ShapeDtypeStruct((ff, width), bf16),
            pltpu.VMEM((toks, PIECE), bf16),
            pltpu.VMEM((toks, PIECE), f32),
        ),
        in_specs=[vmem] * 4,
        out_specs=(hbm,) * 3 + (vmem,) * 2,
        scratch_shapes=[dma((12,))],
        cost_estimate=pl.CostEstimate(flops=6 * 10**9, bytes_accessed=18 * 10**6, transcendentals=0),
        compiler_params=pltpu.CompilerParams(vmem_limit_bytes=12 * 2**20),
    )(W.reshape(2, width, ff), Dn.reshape(ff, width), H, R1)
    mixed = pl.pallas_call(
        add_last,
        out_shape=jax.ShapeDtypeStruct((toks, dcols), bf16),
        in_specs=[vmem] * 4,
        out_specs=hbm,
        scratch_shapes=[pltpu.VMEM((toks, PIECE), bf16), dma((2,))],
        compiler_params=pltpu.CompilerParams(vmem_limit_bytes=8 * 2**20),
    )(done, own, up, down)
    return g_out, u_out, d_out, mixed


def solution(mesh):
    in_specs = (P("fs", None), P("fs"), P("fs", "tp"), P("fs", "tp"), P("fs", "tp"))
    out_specs = (P(None, "tp"), P(None, "tp"), P("tp", None), P("fs", "tp"))
    return jax.shard_map(
        on_device, mesh=mesh, in_specs=in_specs, out_specs=out_specs, check_vma=False
    )
```

time: 90.8 us -> 86.2 us (0.949)
  Pallas kernels: 90 us -> 79.7 us
  waiting for transfers between devices: 0 us -> 2.99 us
  starting transfers between devices: 0 us -> 2.74 us
    pallas_call x1, Pallas kernels: 83.7 us -> 72.7 us  [on_device(): pl.pallas_call(kernel, out_shape=(pltpu.VMEM((2, RING, RING, 2, rows, ff)...]
    ppermute x0 -> x2, waiting for transfers between devices: none -> 2.99 us  [the longest x1 2.99 us: on_device(): up = lax.ppermute(Tp, 'tp', [(i, (i + 1) % RING) for i in range(RING)])]
    ppermute x0 -> x2, starting transfers between devices: none -> 2.74 us  [the longest x1 2.66 us: on_device(): lax.ppermute(Tm, 'tp', [(i, (i + RING - 1) % RING) for i in range(RING)])]
  transfers between devices with their start and end apart: 0 -> 2, of which waited for: 0 -> 1; matrix products, arithmetic and copies ran while one was open for 0% -> 0% of each run, Pallas kernels for 0% -> 7%
where the time goes in v3:
time: 86.2 us; the launch traced here: 86 us
  Pallas kernels  79.7 us (92%)
  waiting for transfers between devices  2.99 us (3%)
  starting transfers between devices  2.74 us (3%)
    pallas_call x1, Pallas kernels, on_device(): pl.pallas_call(kernel, out_shape=(pltpu.VMEM((2, RING, RING, 2, rows, ff)...  72.7 us
    pallas_call x1, Pallas kernels, on_device(): pl.pallas_call(write_out, out_shape=(jax.ShapeDtypeStruct((width, ff), bf...  6.09 us
    ppermute x1, waiting for transfers between devices, on_device(): up = lax.ppermute(Tp, 'tp', [(i, (i + 1) % RING) for i in range(RING)])  2.99 us
    ppermute x1, starting transfers between devices, on_device(): lax.ppermute(Tm, 'tp', [(i, (i + RING - 1) % RING) for i in range(RING)])  2.66 us
  transfers between devices with their start and end apart: 2, of which 1 were waited for; matrix products, arithmetic and copies ran while one was open for 0% of the time, Pallas kernels for 7%

profile of v3, /device:TPU:1, one launch (start us, length us, event | category | flops | bytes accessed | tf_op | source)
XLA Modules:
  0.0 86.0 jit_solution(16978145262054871702)
XLA Ops:
  0.6 72.7 %shard_map.84 = (bf16[2,4,4,2,64,1408]{5,4,3,2,1,0:T(8,128)(2,1)S(1)}, bf16[4,2,176,2048]{3,2,1,0:T(8,128)(2,1)S(1)}, bf16[768,1408]{1,0:T(8,128)(2,1)S(1)}, bf1...) custom-call(bf16[768,2048]{1,0:T(8,128)(2,1)} %tok.1, f32[1,64]{1,0:T(1,128)} %bitcast.5, ...), custom_call_target="tpu_custom_call" | custom-call | tf_op jit(solution)/shard_map/pallas_call | solution.py:347
  73.3 0.1 collective-permute-start
  73.4 2.7 %collective-permute-start.1 = (bf16[768,256]{1,0:T(8,128)(2,1)S(1)}, bf16[768,256]{1,0:T(8,128)(2,1)S(1)}, u32[]{:S(2)}, u32[]{:S(2)}) collective-permute-start(bf16[768,256]{1,0:T(8,128)(2,1)S(1)} %get-tuple-element.25), channel_id=1, source_target_pairs={{0,3},{1,0},{2,1},{3,2},{4,7},{5,4},{6,5},{7,6},{8,11},{9,8},{10,9... | collective-permute-start | bytes 1179656 | tf_op jit(solution)/shard_map/ppermute | solution.py:382
  76.1 6.1 %shard_map.85 = (bf16[2048,1408]{1,0:T(8,128)(2,1)}, bf16[2048,1408]{1,0:T(8,128)(2,1)}, bf16[1408,2048]{1,0:T(8,128)(2,1)}, bf16[768,256]{1,0:T(8,128)(2,1)S(1)}, f32[768,256]{1,0:T(8,128)S(1)}) custom-call(bf16[2,2048,1408]{2,1,0:T(8,128)(2,1)S(1)} %bitcast.3, bf16[1408,2048]{1,0:T(8,128)(2,1)S(1)} %bitcast.4, bf16[768,1408]{1,0:T(8,128)(2,1)S(1)} %get-tuple-element.17.H, ...), custom_call_target="tpu_custom_call" | custom-call | flops 6000000000 | bytes 18000000 | tf_op jit(solution)/shard_map/pallas_call | solution.py:383
  82.2 3.0 %collective-permute-done.up = bf16[768,256]{1,0:T(8,128)(2,1)S(1)} collective-permute-done((bf16[768,256]{1,0:T(8,128)(2,1)S(1)}, bf16[768,256]{1,0:T(8,128)(2,1)S(1)}, u32[]{:S(2)}, u32[]{:S(2)}) %collective-permute-start) | collective-permute-done | bytes 393248 | tf_op jit(solution)/shard_map/ppermute | solution.py:381
  85.1 0.0 collective-permute-done.1.down
  85.1 0.9 %shard_map.86 = bf16[768,512]{1,0:T(8,128)(2,1)} custom-call(bf16[768,256]{1,0:T(8,128)(2,1)S(1)} %get-tuple-element.22.done, f32[768,256]{1,0:T(8,128)S(1)} %get-tuple-element.23.own, bf16[768,256]{1,0:T(8,128)(2,1)S(1)} %collective-permute-done.up, bf16[768,256]{1,0:T(8,128)(2,1)S(1)} %collective-permute-done.1.down), custom_call_target="tpu_custom_call" | custom-call | tf_op jit(solution)/shard_map/pallas_call | solution.py:398
Async XLA Ops:
  73.3 11.8 %collective-permute-start = (bf16[768,256]{1,0:T(8,128)(2,1)S(1)}, bf16[768,256]{1,0:T(8,128)(2,1)S(1)}, u32[]{:S(2)}, u32[]{:S(2)}) collective-permute-start(bf16[768,256]{1,0:T(8,128)(2,1)S(1)} %get-tuple-element.24), channel_id=1, source_target_pairs={{0,1},{1,2},{2,3},{3,0},{4,5},{5,6},{6,7},{7,4},{8,9},{9,10},{10,1... | collective-permute-start | bytes 1179656 | tf_op jit(solution)/shard_map/ppermute | solution.py:381
  73.4 11.8 %collective-permute-start.1 = (bf16[768,256]{1,0:T(8,128)(2,1)S(1)}, bf16[768,256]{1,0:T(8,128)(2,1)S(1)}, u32[]{:S(2)}, u32[]{:S(2)}) collective-permute-start(bf16[768,256]{1,0:T(8,128)(2,1)S(1)} %get-tuple-element.25), channel_id=1, source_target_pairs={{0,3},{1,0},{2,1},{3,2},{4,7},{5,4},{6,5},{7,6},{8,11},{9,8},{10,9... | collective-permute-start | bytes 1179656 | tf_op jit(solution)/shard_map/ppermute | solution.py:382

commit v4 on v3

--- a/solution.py
+++ b/solution.py
@@ -9,7 +9,7 @@
 bf16, f32 = jnp.bfloat16, jnp.float32
 eps_norm = 1e-06
 RING = 4
-CHUNKS = ((0, 384), (384, 256), (640, 256), (896, 256), (1152, 256))
+CHUNKS = ((0, 256), (256, 256), (512, 256), (768, 256), (1024, 256), (1280, 128))
 NCH = len(CHUNKS)
 PARTS = 2
 PIECE = 256
@@ -17,18 +17,19 @@
 NP = len(OFFS)
 TILE = 256
 ORDER = (
-    "P1S.0", "P1S.1", "P1S.2", "P2S.0.0", "P1S.3", "P2S.4.0", "P2S.3.0", "D0S.0", "NORM.0", "P1S.4",
-    "P1F.0", "P1F.2", "P2S.2.3", "P2S.0.3", "P1F.4", "P2S.2.0", "P1E.0", "P1E.2", "D0S.1", "P1F.3",
-    "P2S.0.1", "P2S.4.1", "NORM.1", "P2S.2.1", "P2S.0.2", "D0.0", "P1F.1", "NORM.2", "P2S.1.3", "D1S.0",
-    "P1E.4", "P2S.4.2", "P2S.4.3", "P1E.1", "P2S.2.2", "P2F.0", "P2S.1.1", "D0.1", "D1F.0", "P2S.1.2",
-    "D1S.1", "P2S.3.3", "P2E.0", "P2S.1.0", "P2F.4", "P2S.3.1", "P1E.3", "P2S.3.2", "D1E.0", "D1F.1",
-    "D2S.0", "P2F.2", "HID.0.0", "P2E.4", "D1E.1", "D1S.2", "D2S.1", "P2F.3", "HID.0.1", "P2E.2", "D1S.3",
-    "D2F.0", "P2F.1", "HID.4.0", "D1S.4", "D1F.2", "HID.4.1", "HID.2.0", "D2F.1", "P2E.3", "D1S.5",
-    "HID.2.1", "D1F.3", "D1E.2", "D2S.2", "D2E.0", "HID.3.0", "P2E.1", "HID.3.1", "D1S.6", "D1S.7", "D1E.3",
-    "D2S.3", "D2E.1", "HID.1.0", "HID.1.1", "D1F.4", "SH.0", "D1F.5", "D2F.2", "SH.1", "D2F.3", "D1E.4",
-    "D2S.4", "D1F.6", "D1F.7", "D2E.2", "D1E.5", "D2S.5", "D2E.3", "D1E.6", "D2S.6", "SH.2", "SH.3",
-    "D2F.4", "D1E.7", "D2S.7", "D2F.5", "D2F.6", "D2E.4", "D2F.7", "SH.4", "D2E.5", "D2E.6", "D2E.7",
-    "SH.5", "SH.6", "SH.7",
+    "P1S.0", "P1S.1", "NORM.0", "D0S.0", "P1S.2", "P2S.0.0", "P1S.3", "P1S.4", "P1F.1", "P1F.0", "P2S.5.0",
+    "P2S.1.1", "P2S.1.0", "P1S.5", "P1F.3", "P1F.4", "P2S.1.3", "P2S.4.1", "D0.0", "P2S.0.3", "D1S.0",
+    "P1F.5", "P1E.1", "P1E.4", "D0S.1", "P2S.3.0", "P2S.4.3", "NORM.1", "P2S.1.2", "P2S.4.0", "P2S.5.3",
+    "P2S.4.2", "P1E.0", "P2S.0.2", "P1E.5", "P1E.3", "P2S.5.1", "P1F.2", "P2S.3.1", "P2S.5.2", "D0.1",
+    "P2S.2.0", "D1F.0", "D1S.1", "P2F.4", "P1E.2", "P2S.0.1", "P2F.5", "P2S.3.3", "NORM.2", "P2F.1",
+    "D1F.1", "P2S.2.1", "P2S.2.3", "P2E.4", "P2S.2.2", "P2E.5", "P2F.0", "D1E.0", "D2S.0", "P2S.3.2",
+    "HID.4.0", "HID.5.0", "D1S.2", "P2E.1", "HID.4.1", "D1E.1", "D2S.1", "P2F.2", "HID.1.0", "P2E.0",
+    "D2F.0", "HID.5.1", "D1S.3", "P2F.3", "D1F.2", "D1S.4", "D1S.5", "HID.0.0", "D2F.1", "P2E.2", "HID.1.1",
+    "HID.0.1", "D1S.6", "D1F.3", "D1E.2", "D2S.2", "D2E.0", "HID.2.0", "P2E.3", "HID.2.1", "D1E.3", "D2S.3",
+    "D2E.1", "D1F.4", "D1S.7", "HID.3.0", "SHA.0", "HID.3.1", "D2F.2", "D1F.5", "SHA.1", "D1E.4", "D2F.3",
+    "D2S.4", "D1F.6", "SH.1", "D2E.2", "D1F.7", "D1E.5", "D2S.5", "D2E.3", "D1E.6", "D2S.6", "SH.2",
+    "D1E.7", "D2S.7", "SH.3", "D2F.4", "D2F.5", "D2F.6", "D2F.7", "D2E.4", "D2E.5", "D2E.6", "D2E.7",
+    "SH.4", "SH.5", "SH.6", "SH.7",
 )
 
 
@@ -235,8 +236,12 @@
         if i == 0:
             sent(Dn.at[:, c], out_sem.at[9])
 
-    def SH(i):
-        arrived(Dn.at[:, 1 - c, :, piece_cols(i)], d_sem.at[4, i])
+    def SHA(t):
+        SH(0, t)
+
+    def SH(i, part=None):
+        if not part:
+            arrived(Dn.at[:, 1 - c, :, piece_cols(i)], d_sem.at[4, i])
         off, p = OFFS[i]
         if off == 0:
             return
@@ -247,7 +252,8 @@
             arrived(R2.at[p, d], r2_sem.at[p, d])
 
         def body(t, _):
-            at_rows = pl.ds(pl.multiple_of(t * TILE, TILE), TILE)
+            tile = TILE if part is None else H.shape[0] // PARTS
+            at_rows = pl.ds(pl.multiple_of(t * tile, tile), tile)
             w = Dn[:, :, :, cols].reshape(-1, PIECE)
             v = jnp.dot(H[at_rows, :], w, preferred_element_type=f32)
             if off == 2:
@@ -267,8 +273,11 @@
                 copy(S1.at[d, at_rows, :], R1.at[d, at_rows, :], out_sem.at[11], r1_sem.at[0], xnear[d]).start()
             return 0
 
-        lax.fori_loop(0, H.shape[0] // TILE, body, 0)
-        if i == 0:
+        if part is None:
+            lax.fori_loop(0, H.shape[0] // TILE, body, 0)
+        else:
+            body(part, 0)
+        if i == 1:
             sent(S2, out_sem.at[10])
             sent(S1, out_sem.at[11])
 
@@ -287,7 +296,7 @@
 
         lax.fori_loop(0, count, body, 0)
 
-    does = {f.__name__: f for f in (P1S, P1F, P1E, P2S, P2F, P2E, HID, NORM, D0S, D0, D1S, D1F, D1E, D2S, D2F, D2E, SH)}
+    does = {f.__name__: f for f in (P1S, P1F, P1E, P2S, P2F, P2E, HID, NORM, D0S, D0, D1S, D1F, D1E, D2S, D2F, D2E, SH, SHA)}
     for word in ORDER:
         name, *numbers = word.split(".")
         does[name](*map(int, numbers))

time: 86.2 us -> 83.9 us (0.973)
  Pallas kernels: 79.7 us -> 77.8 us
    pallas_call x1, Pallas kernels: 72.7 us -> 70.8 us  [on_device(): pl.pallas_call(kernel, out_shape=(pltpu.VMEM((2, RING, RING, 2, rows, ff)...]
where the time goes in v4:
time: 83.9 us; the launch traced here: 83.4 us
  Pallas kernels  77.8 us (93%)
  starting transfers between devices  2.74 us (3%)
  waiting for transfers between devices  2.26 us (3%)
    pallas_call x1, Pallas kernels, on_device(): pl.pallas_call(kernel, out_shape=(pltpu.VMEM((2, RING, RING, 2, rows, ff)...  70.8 us
    pallas_call x1, Pallas kernels, on_device(): pl.pallas_call(write_out, out_shape=(jax.ShapeDtypeStruct((width, ff), bf...  6.09 us
    ppermute x1, starting transfers between devices, on_device(): lax.ppermute(Tm, 'tp', [(i, (i + RING - 1) % RING) for i in range(RING)])  2.66 us
    ppermute x1, waiting for transfers between devices, on_device(): up = lax.ppermute(Tp, 'tp', [(i, (i + 1) % RING) for i in range(RING)])  2.26 us
  transfers between devices with their start and end apart: 2, of which 1 were waited for; matrix products, arithmetic and copies ran while one was open for 0% of the time, Pallas kernels for 7%

profile of v4, /device:TPU:1, one launch (start us, length us, event | category | flops | bytes accessed | tf_op | source)
XLA Modules:
  0.0 83.4 jit_solution(18130315277110998759)
XLA Ops:
  0.6 70.8 %shard_map.84 = (bf16[2,4,4,2,64,1408]{5,4,3,2,1,0:T(8,128)(2,1)S(1)}, bf16[4,2,176,2048]{3,2,1,0:T(8,128)(2,1)S(1)}, bf16[768,1408]{1,0:T(8,128)(2,1)S(1)}, bf1...) custom-call(bf16[768,2048]{1,0:T(8,128)(2,1)} %tok.1, f32[1,64]{1,0:T(1,128)} %bitcast.5, ...), custom_call_target="tpu_custom_call" | custom-call | tf_op jit(solution)/shard_map/pallas_call | solution.py:356
  71.4 0.1 collective-permute-start
  71.5 2.7 %collective-permute-start.1 = (bf16[768,256]{1,0:T(8,128)(2,1)S(1)}, bf16[768,256]{1,0:T(8,128)(2,1)S(1)}, u32[]{:S(2)}, u32[]{:S(2)}) collective-permute-start(bf16[768,256]{1,0:T(8,128)(2,1)S(1)} %get-tuple-element.25), channel_id=1, source_target_pairs={{0,3},{1,0},{2,1},{3,2},{4,7},{5,4},{6,5},{7,6},{8,11},{9,8},{10,9... | collective-permute-start | bytes 1179656 | tf_op jit(solution)/shard_map/ppermute | solution.py:391
  74.2 6.1 %shard_map.85 = (bf16[2048,1408]{1,0:T(8,128)(2,1)}, bf16[2048,1408]{1,0:T(8,128)(2,1)}, bf16[1408,2048]{1,0:T(8,128)(2,1)}, bf16[768,256]{1,0:T(8,128)(2,1)S(1)}, f32[768,256]{1,0:T(8,128)S(1)}) custom-call(bf16[2,2048,1408]{2,1,0:T(8,128)(2,1)S(1)} %bitcast.3, bf16[1408,2048]{1,0:T(8,128)(2,1)S(1)} %bitcast.4, bf16[768,1408]{1,0:T(8,128)(2,1)S(1)} %get-tuple-element.17.H, ...), custom_call_target="tpu_custom_call" | custom-call | flops 6000000000 | bytes 18000000 | tf_op jit(solution)/shard_map/pallas_call | solution.py:392
  80.3 2.3 %collective-permute-done.up = bf16[768,256]{1,0:T(8,128)(2,1)S(1)} collective-permute-done((bf16[768,256]{1,0:T(8,128)(2,1)S(1)}, bf16[768,256]{1,0:T(8,128)(2,1)S(1)}, u32[]{:S(2)}, u32[]{:S(2)}) %collective-permute-start) | collective-permute-done | bytes 393248 | tf_op jit(solution)/shard_map/ppermute | solution.py:390
  82.5 0.0 collective-permute-done.1.down
  82.5 0.9 %shard_map.86 = bf16[768,512]{1,0:T(8,128)(2,1)} custom-call(bf16[768,256]{1,0:T(8,128)(2,1)S(1)} %get-tuple-element.22.done, f32[768,256]{1,0:T(8,128)S(1)} %get-tuple-element.23.own, bf16[768,256]{1,0:T(8,128)(2,1)S(1)} %collective-permute-done.up, bf16[768,256]{1,0:T(8,128)(2,1)S(1)} %collective-permute-done.1.down), custom_call_target="tpu_custom_call" | custom-call | tf_op jit(solution)/shard_map/pallas_call | solution.py:407
Async XLA Ops:
  71.4 11.1 %collective-permute-start = (bf16[768,256]{1,0:T(8,128)(2,1)S(1)}, bf16[768,256]{1,0:T(8,128)(2,1)S(1)}, u32[]{:S(2)}, u32[]{:S(2)}) collective-permute-start(bf16[768,256]{1,0:T(8,128)(2,1)S(1)} %get-tuple-element.24), channel_id=1, source_target_pairs={{0,1},{1,2},{2,3},{3,0},{4,5},{5,6},{6,7},{7,4},{8,9},{9,10},{10,1... | collective-permute-start | bytes 1179656 | tf_op jit(solution)/shard_map/ppermute | solution.py:390
  71.5 11.0 %collective-permute-start.1 = (bf16[768,256]{1,0:T(8,128)(2,1)S(1)}, bf16[768,256]{1,0:T(8,128)(2,1)S(1)}, u32[]{:S(2)}, u32[]{:S(2)}) collective-permute-start(bf16[768,256]{1,0:T(8,128)(2,1)S(1)} %get-tuple-element.25), channel_id=1, source_target_pairs={{0,3},{1,0},{2,1},{3,2},{4,7},{5,4},{6,5},{7,6},{8,11},{9,8},{10,9... | collective-permute-start | bytes 1179656 | tf_op jit(solution)/shard_map/ppermute | solution.py:391

commit v5 on v4

--- a/solution.py
+++ b/solution.py
@@ -308,7 +308,7 @@
             pl.when(cond)(d.wait_send)
 
 
-def write_out(W, Dn, H, R1, g_out, u_out, d_out, done, own, sem):
+def write_out(W, Dn, H, R1, g_out, u_out, d_out, m_out, own, done, sem):
     x = lax.axis_index("tp")
     ff, width = d_out.shape
     dcols = width // RING
@@ -331,16 +331,19 @@
         return 0
 
     lax.fori_loop(0, H.shape[0] // TILE, body, 0)
+    copies.append(pltpu.make_async_copy(done, m_out.at[:, pl.ds(0, PIECE)], sem.at[len(copies)]))
+    copies[-1].start()
     for cp in copies:
         cp.wait()
 
 
-def add_last(done, own, up, down, m_out, last, sem):
-    copies = [pltpu.make_async_copy(done, m_out.at[:, pl.ds(0, PIECE)], sem.at[0]),
-              pltpu.make_async_copy(last, m_out.at[:, pl.ds(PIECE, PIECE)], sem.at[1])]
-    copies[0].start()
-    last[...] = (own[...] + up[...].astype(f32) + down[...].astype(f32)).astype(bf16)
-    copies[1].start()
+def add_last(m_in, own, up, down, m_out, last, sem):
+    copies = []
+    for t in range(own.shape[0] // TILE):
+        r = pl.ds(t * TILE, TILE)
+        last[r, :] = (own[r, :] + up[r, :].astype(f32) + down[r, :].astype(f32)).astype(bf16)
+        copies.append(pltpu.make_async_copy(last.at[r], m_out.at[r, pl.ds(PIECE, PIECE)], sem.at[t]))
+        copies[-1].start()
     for cp in copies:
         cp.wait()
 
@@ -389,29 +392,30 @@
     )(tokens, norm_gain.reshape(1, rows), gate_weight, up_weight, down_weight)
     up = lax.ppermute(Tp, "tp", [(i, (i + 1) % RING) for i in range(RING)])
     down = lax.ppermute(Tm, "tp", [(i, (i + RING - 1) % RING) for i in range(RING)])
-    g_out, u_out, d_out, done, own = pl.pallas_call(
+    g_out, u_out, d_out, half, own = pl.pallas_call(
         write_out,
         out_shape=(
             jax.ShapeDtypeStruct((width, ff), bf16),
             jax.ShapeDtypeStruct((width, ff), bf16),
             jax.ShapeDtypeStruct((ff, width), bf16),
-            pltpu.VMEM((toks, PIECE), bf16),
+            jax.ShapeDtypeStruct((toks, dcols), bf16),
             pltpu.VMEM((toks, PIECE), f32),
         ),
         in_specs=[vmem] * 4,
-        out_specs=(hbm,) * 3 + (vmem,) * 2,
-        scratch_shapes=[dma((12,))],
+        out_specs=(hbm,) * 4 + (vmem,),
+        scratch_shapes=[pltpu.VMEM((toks, PIECE), bf16), dma((13,))],
         cost_estimate=pl.CostEstimate(flops=6 * 10**9, bytes_accessed=18 * 10**6, transcendentals=0),
         compiler_params=pltpu.CompilerParams(vmem_limit_bytes=12 * 2**20),
     )(W.reshape(2, width, ff), Dn.reshape(ff, width), H, R1)
     mixed = pl.pallas_call(
         add_last,
         out_shape=jax.ShapeDtypeStruct((toks, dcols), bf16),
-        in_specs=[vmem] * 4,
+        in_specs=[hbm] + [vmem] * 3,
         out_specs=hbm,
-        scratch_shapes=[pltpu.VMEM((toks, PIECE), bf16), dma((2,))],
+        input_output_aliases={0: 0},
+        scratch_shapes=[pltpu.VMEM((toks, PIECE), bf16), dma((3,))],
         compiler_params=pltpu.CompilerParams(vmem_limit_bytes=8 * 2**20),
-    )(done, own, up, down)
+    )(half, own, up, down)
     return g_out, u_out, d_out, mixed
 
 

time: 83.9 us -> 83.9 us (level)
  no operation moved by 1% of the time
where the time goes in v5:
time: 83.9 us; the launch traced here: 83.4 us
  Pallas kernels  77.8 us (93%)
  starting transfers between devices  2.74 us (3%)
  waiting for transfers between devices  2.18 us (3%)
    pallas_call x1, Pallas kernels, on_device(): pl.pallas_call(kernel, out_shape=(pltpu.VMEM((2, RING, RING, 2, rows, ff)...  70.8 us
    pallas_call x1, Pallas kernels, on_device(): pl.pallas_call(write_out, out_shape=(jax.ShapeDtypeStruct((width, ff), bf...  6.18 us
    ppermute x1, starting transfers between devices, on_device(): lax.ppermute(Tm, 'tp', [(i, (i + RING - 1) % RING) for i in range(RING)])  2.66 us
    ppermute x1, waiting for transfers between devices, on_device(): up = lax.ppermute(Tp, 'tp', [(i, (i + 1) % RING) for i in range(RING)])  2.17 us
  transfers between devices with their start and end apart: 2, of which 1 were waited for; matrix products, arithmetic and copies ran while one was open for 0% of the time, Pallas kernels for 7%

profile of v5, /device:TPU:1, one launch (start us, length us, event | category | flops | bytes accessed | tf_op | source)
XLA Modules:
  0.0 83.4 jit_solution(15462238811414477428)
XLA Ops:
  0.6 70.8 %shard_map.84 = (bf16[2,4,4,2,64,1408]{5,4,3,2,1,0:T(8,128)(2,1)S(1)}, bf16[4,2,176,2048]{3,2,1,0:T(8,128)(2,1)S(1)}, bf16[768,1408]{1,0:T(8,128)(2,1)S(1)}, bf1...) custom-call(bf16[768,2048]{1,0:T(8,128)(2,1)} %tok.1, f32[1,64]{1,0:T(1,128)} %bitcast.5, ...), custom_call_target="tpu_custom_call" | custom-call | tf_op jit(solution)/shard_map/pallas_call | solution.py:359
  71.4 0.1 collective-permute-start
  71.5 2.7 %collective-permute-start.1 = (bf16[768,256]{1,0:T(8,128)(2,1)S(1)}, bf16[768,256]{1,0:T(8,128)(2,1)S(1)}, u32[]{:S(2)}, u32[]{:S(2)}) collective-permute-start(bf16[768,256]{1,0:T(8,128)(2,1)S(1)} %get-tuple-element.25), channel_id=1, source_target_pairs={{0,3},{1,0},{2,1},{3,2},{4,7},{5,4},{6,5},{7,6},{8,11},{9,8},{10,9... | collective-permute-start | bytes 1179656 | tf_op jit(solution)/shard_map/ppermute | solution.py:394
  74.2 6.2 %shard_map.85 = (bf16[2048,1408]{1,0:T(8,128)(2,1)}, bf16[2048,1408]{1,0:T(8,128)(2,1)}, bf16[1408,2048]{1,0:T(8,128)(2,1)}, bf16[768,512]{1,0:T(8,128)(2,1)}, f32[768,256]{1,0:T(8,128)S(1)}) custom-call(bf16[2,2048,1408]{2,1,0:T(8,128)(2,1)S(1)} %bitcast.3, bf16[1408,2048]{1,0:T(8,128)(2,1)S(1)} %bitcast.4, bf16[768,1408]{1,0:T(8,128)(2,1)S(1)} %get-tuple-element.17.H, ...), custom_call_target="tpu_custom_call" | custom-call | flops 6000000000 | bytes 18000000 | tf_op jit(solution)/shard_map/pallas_call | solution.py:395
  80.4 2.2 %collective-permute-done.up = bf16[768,256]{1,0:T(8,128)(2,1)S(1)} collective-permute-done((bf16[768,256]{1,0:T(8,128)(2,1)S(1)}, bf16[768,256]{1,0:T(8,128)(2,1)S(1)}, u32[]{:S(2)}, u32[]{:S(2)}) %collective-permute-start) | collective-permute-done | bytes 393248 | tf_op jit(solution)/shard_map/ppermute | solution.py:393
  82.5 0.0 collective-permute-done.1.down
  82.5 0.8 shard_map.86
Async XLA Ops:
  71.4 11.1 %collective-permute-start = (bf16[768,256]{1,0:T(8,128)(2,1)S(1)}, bf16[768,256]{1,0:T(8,128)(2,1)S(1)}, u32[]{:S(2)}, u32[]{:S(2)}) collective-permute-start(bf16[768,256]{1,0:T(8,128)(2,1)S(1)} %get-tuple-element.24), channel_id=1, source_target_pairs={{0,1},{1,2},{2,3},{3,0},{4,5},{5,6},{6,7},{7,4},{8,9},{9,10},{10,1... | collective-permute-start | bytes 1179656 | tf_op jit(solution)/shard_map/ppermute | solution.py:393
  71.5 11.0 %collective-permute-start.1 = (bf16[768,256]{1,0:T(8,128)(2,1)S(1)}, bf16[768,256]{1,0:T(8,128)(2,1)S(1)}, u32[]{:S(2)}, u32[]{:S(2)}) collective-permute-start(bf16[768,256]{1,0:T(8,128)(2,1)S(1)} %get-tuple-element.25), channel_id=1, source_target_pairs={{0,3},{1,0},{2,1},{3,2},{4,7},{5,4},{6,5},{7,6},{8,11},{9,8},{10,9... | collective-permute-start | bytes 1179656 | tf_op jit(solution)/shard_map/ppermute | solution.py:394
